TPU v7x, 32 devices: a whole 2x2x4 slice. The times are simulated.
32 devices in a mesh: sp: 8 (over z, y), dp: 4 (over x, core).
Axes of the slice: x: 2, y: 2, z: 4, core: 2. Of those that a mesh axis runs over, the one named last changes fastest.
Arguments:
- stream: bfloat16 [4, 1024, 2048], P('dp', 'sp'), may hold values from -6 to 6
- queries: bfloat16 [4, 1024, 1024], P('dp', 'sp'), may hold values from -6 to 6
- keys_in: bfloat16 [4, 1024, 1024], P('dp', 'sp'), may hold values from -6 to 6
- values_in: bfloat16 [4, 1024, 1024], P('dp', 'sp'), may hold values from -6 to 6
- key_shift: bfloat16 [4, 1024, 16], P('dp', 'sp'), may hold values from -8 to 16
- head_shift: float32 [16], replicated, may hold values from -16 to 0
- mix_gain: float32 [1024], replicated, may hold values from 0.1 to 1.9
- out_weight: bfloat16 [1024, 2048], replicated, may hold values from -0.1875 to 0.1875
- post_gain: float32 [2048], replicated, may hold values from 0.1 to 1.9
- route: int32 [4, 1024, 2], P('dp', 'sp'), may hold values from 0 to 31, as said below
- route_weight: float32 [4, 1024, 2], P('dp', 'sp'), may hold values from 0.25 to 1
- w_gate: bfloat16 [32, 2048, 1024], P(('sp', 'dp')), may hold values from -0.125 to 0.125
- w_up: bfloat16 [32, 2048, 1024], P(('sp', 'dp')), may hold values from -0.125 to 0.125
- w_down: bfloat16 [32, 1024, 2048], P(('sp', 'dp')), may hold values from -0.1875 to 0.1875
Outputs:
- result: bfloat16 [4, 1024, 2048], P('dp', 'sp')
Inputs may be any that keep to these rules, and one draw needn't show every extreme that they name: `route`: each token names two different experts of one group (the group of expert e is e // 8). Of the 128 tokens of one device, each expert is named by at most 16; in every draw the 8 experts of one group are each named by exactly 16 tokens of every device.
All inputs are finite; a program needn't handle non-finite values.
Results may differ from a plain program's by a relative error of at most 0.0085.
Values may be sent and summed in bfloat16 or wider, within the bound.
No kernel may reach another device: no remote copies, remote signals or barrier semaphores. Data moves between devices by JAX's collectives and lax.ppermute only.
A program may use at most 128 MiB of HBM per device.

v0:
```python
import functools
import math

import jax
import jax.numpy as jnp
from jax import lax
from jax.experimental import pallas as pl
from jax.experimental.pallas import tpu as pltpu
from jax.sharding import PartitionSpec as P

HD = 64
GROUPS = 4
norm_eps = 1e-05
F32 = jnp.float32
BF16 = jnp.bfloat16
MB = 1024 * 1024

VM = pl.BlockSpec(memory_space=pltpu.VMEM)
SM = pl.BlockSpec(memory_space=pltpu.SMEM)
NT = (((1,), (1,)), ((), ()))


def call(body, out, n_in, scratch=(), limit=40, in_specs=None, flops=0, name=None):
    return pl.pallas_call(
        body,
        out_shape=out,
        in_specs=in_specs or [VM] * n_in,
        out_specs=jax.tree.map(lambda _: VM, out),
        scratch_shapes=list(scratch),
        compiler_params=pltpu.CompilerParams(vmem_limit_bytes=limit * MB),
        cost_estimate=pl.CostEstimate(flops=flops, bytes_accessed=MB, transcendentals=0),
        name=name,
    )


def iota(shape, dim):
    return lax.broadcasted_iota(jnp.int32, shape, dim)


def pack_body(q_ref, k_ref, v_ref, ks_ref, out_ref):
    n, rows, cols = out_ref.shape
    tokens, heads = ks_ref.shape[1], ks_ref.shape[2]
    local = heads // n
    pieces = tokens // cols
    eye = (iota((heads, heads), 0) == iota((heads, heads), 1)).astype(BF16)
    shift = lax.dot_general(eye, ks_ref[0], NT, preferred_element_type=F32)
    pad = rows - 3 * tokens
    for d in range(n):
        lanes = slice(d * cols, (d + 1) * cols)
        out_ref[d, 0:tokens, :] = q_ref[0, :, lanes]
        out_ref[d, tokens : 2 * tokens, :] = k_ref[0, :, lanes]
        out_ref[d, 2 * tokens : 3 * tokens, :] = v_ref[0, :, lanes]
        tail = [
            shift[d * local + h : d * local + h + 1, p * cols : (p + 1) * cols]
            for h in range(local)
            for p in range(pieces)
        ]
        tail.append(jnp.zeros((pad - len(tail), cols), F32))
        out_ref[d, 3 * tokens :, :] = jnp.concatenate(tail, axis=0).astype(BF16)


def attention_body(hs_ref, x_ref, out_ref, z_ref, w_ref):
    n, _, cols = x_ref.shape
    tokens = out_ref.shape[1]
    local = cols // HD
    pieces = tokens // cols
    lane = iota((tokens, cols), 1) // HD
    keys = x_ref[:, tokens : 2 * tokens, :].reshape(n * tokens, cols)
    values = x_ref[:, 2 * tokens : 3 * tokens, :].reshape(n * tokens, cols)
    row, col = iota((2 * tokens, 2 * tokens), 0), iota((2 * tokens, 2 * tokens), 1)
    summing = jnp.where((col >= tokens) | (row % tokens >= col), 1.0, 0.0).astype(BF16)
    causal = iota((tokens, tokens), 1) < iota((tokens, tokens), 0)
    for i in range(n):
        total = None
        for h in range(local):
            q = x_ref[i, 0:tokens, :].astype(F32) * (1.0 / math.sqrt(HD))
            q = jnp.where(lane == h, q, 0.0).astype(BF16)
            span = (i + 1) * tokens
            z_ref[h, :, 0:span] = lax.dot_general(
                q, keys[0:span], NT, preferred_element_type=F32
            )
            carry = None
            for j in range(i, -1, -1):
                at = slice(j * tokens, (j + 1) * tokens)
                base = 3 * tokens + h * pieces
                off = [x_ref[j, base + p : base + p + 1, :] for p in range(pieces)]
                off = off[0] if pieces == 1 else jnp.concatenate(off, axis=1)
                z = z_ref[h, :, at] + (off.astype(F32) + hs_ref[h])
                breaks = -(jnp.maximum(z, 0.0) + jnp.log(1.0 + jnp.exp(-jnp.abs(z))))
                if j == i:
                    breaks = jnp.where(causal, breaks, 0.0)
                high = breaks.astype(BF16)
                low = (breaks - high.astype(F32)).astype(BF16)
                sums = jnp.dot(
                    jnp.concatenate([high, low], axis=1), summing, preferred_element_type=F32
                )
                power = z + sums[:, 0:tokens]
                if carry is not None:
                    power = power + carry
                weight = jnp.exp(power)
                if j == i:
                    weight = jnp.where(causal, weight, 0.0)
                w_ref[h, :, at] = weight.astype(BF16)
                part = sums[:, tokens:]
                carry = part if carry is None else carry + part
            got = jnp.dot(w_ref[h, :, 0:span], values[0:span], preferred_element_type=F32)
            total = got if total is None else jnp.where(lane == h, got, total)
        out_ref[i] = total.astype(BF16)


def route_body(route_ref, row_ref, col_ref, *, n_expert, capacity):
    tokens = route_ref.shape[1]
    ids = route_ref[0].astype(F32)
    eye = iota((tokens, tokens), 0) == iota((tokens, tokens), 1)
    before = (iota((tokens, tokens), 0) < iota((tokens, tokens), 1)).astype(BF16)
    e_rows = [
        jnp.sum(jnp.where(eye, ids[:, k : k + 1], 0.0), axis=0, keepdims=True) for k in range(2)
    ]
    names = iota((n_expert, tokens), 0).astype(F32)
    hot = [(names == e).astype(F32) for e in e_rows]
    earlier = jnp.dot((hot[0] + hot[1]).astype(BF16), before, preferred_element_type=F32)
    rows, cols = [], []
    for k in range(2):
        rank = jnp.sum(hot[k] * earlier, axis=0, keepdims=True)
        dest = e_rows[k] * capacity + rank
        rows.append(dest)
        cols.append(jnp.sum(jnp.where(eye, dest, 0.0), axis=1, keepdims=True))
    row_ref[...] = jnp.concatenate(rows + [jnp.zeros((6, tokens), F32)], axis=0).astype(jnp.int32)
    lane = iota((tokens, 128), 1)
    col_ref[...] = jnp.where(lane == 0, cols[0], cols[1]).astype(jnp.int32)


def hidden_body(att_ref, stream_ref, mg_ref, w_ref, pg_ref, dest_ref, hid_ref, send_ref):
    n, tokens, cols = att_ref.shape
    pieces = [att_ref[s].astype(F32) for s in range(n)]
    if cols % 128 == 0:
        pieces = [jnp.concatenate(pieces, axis=1)]
    size = pieces[0].shape[1]
    square = sum(jnp.sum(p * p, axis=1, keepdims=True) for p in pieces)
    scale = lax.rsqrt(square / (n * cols) + norm_eps)
    mixed = None
    for s, p in enumerate(pieces):
        at = slice(s * size, (s + 1) * size)
        normed = (p * scale * mg_ref[:, at]).astype(BF16)
        part = jnp.dot(normed, w_ref[at, :], preferred_element_type=F32)
        mixed = part if mixed is None else mixed + part
    summed = stream_ref[0].astype(F32) + mixed
    mean = jnp.mean(summed * summed, axis=1, keepdims=True)
    hidden = (summed * lax.rsqrt(mean + norm_eps) * pg_ref[...]).astype(BF16)
    hid_ref[...] = hidden
    total = send_ref.shape[0]
    slot = iota((total, tokens), 0)
    pick = (slot == dest_ref[0:1, :]) | (slot == dest_ref[1:2, :])
    send_ref[...] = jnp.dot(
        pick.astype(F32).astype(BF16), hidden, preferred_element_type=F32
    ).astype(BF16)


def expert_body(x_ref, wg_ref, wu_ref, wd_ref, out_ref, acc_ref):
    step = pl.program_id(0)
    x = x_ref[...]
    gate = jnp.dot(x, wg_ref[0], preferred_element_type=F32)
    upper = jnp.dot(x, wu_ref[0], preferred_element_type=F32)
    inner = (gate / (1.0 + jnp.exp(-gate)) * upper).astype(BF16)
    part = jnp.dot(inner, wd_ref[0], preferred_element_type=F32)

    @pl.when(step == 0)
    def _():
        acc_ref[...] = part

    @pl.when(step > 0)
    def _():
        acc_ref[...] += part

    @pl.when(step == pl.num_programs(0) - 1)
    def _():
        out_ref[...] = acc_ref[...].astype(BF16)


def combine_body(ret_ref, hid_ref, rw_ref, dest_ref, out_ref):
    tokens = hid_ref.shape[0]
    total = ret_ref.shape[0]
    slot = iota((tokens, total), 1)
    result = hid_ref[...].astype(F32)
    for k in range(2):
        pick = (slot == dest_ref[:, k : k + 1]).astype(F32).astype(BF16)
        rows = jnp.dot(pick, ret_ref[...], preferred_element_type=F32)
        result = result + rows * rw_ref[0, :, k : k + 1]
    out_ref[0] = result.astype(BF16)


def on_device(
    stream,
    queries,
    keys_in,
    values_in,
    key_shift,
    head_shift,
    mix_gain,
    out_weight,
    post_gain,
    route,
    route_weight,
    w_gate,
    w_up,
    w_down,
):
    tokens, width = stream.shape[1], stream.shape[2]
    size_sp, size_dp = lax.axis_size("sp"), lax.axis_size("dp")
    heads = key_shift.shape[2]
    local = heads // size_sp
    cols = queries.shape[2] // size_sp
    rows = 3 * tokens + 16
    n_expert = size_sp * size_dp
    capacity = tokens // (n_expert // GROUPS)
    slots = n_expert * capacity
    sds = jax.ShapeDtypeStruct

    sent = call(pack_body, sds((size_sp, rows, cols), BF16), 4, name="pack")(
        queries, keys_in, values_in, key_shift
    )
    got = lax.all_to_all(sent, "sp", split_axis=0, concat_axis=0, tiled=True)
    dest_rows, dest_cols = call(
        functools.partial(route_body, n_expert=n_expert, capacity=capacity),
        (sds((8, tokens), jnp.int32), sds((tokens, 128), jnp.int32)),
        1,
        name="route",
    )(route)
    own_shift = lax.dynamic_slice_in_dim(head_shift, lax.axis_index("sp") * local, local)
    seq = size_sp * tokens
    att = call(
        attention_body,
        sds((size_sp, tokens, cols), BF16),
        2,
        in_specs=[SM, VM],
        scratch=[pltpu.VMEM((local, tokens, seq), F32), pltpu.VMEM((local, tokens, seq), BF16)],
        name="attention",
    )(own_shift, got)
    att = lax.all_to_all(att, "sp", split_axis=0, concat_axis=0, tiled=True)
    hidden, send = call(
        hidden_body,
        (sds((tokens, width), BF16), sds((slots, width), BF16)),
        6,
        name="hidden",
    )(att, stream, mix_gain[None], out_weight, post_gain[None], dest_rows)
    received = lax.all_to_all(
        send.reshape(n_expert, capacity, width),
        ("sp", "dp"),
        split_axis=0,
        concat_axis=0,
        tiled=True,
    ).reshape(slots, width)
    f = w_gate.shape[2]
    step = min(256, f)
    reply = pl.pallas_call(
        expert_body,
        grid=(f // step,),
        out_shape=sds((slots, width), BF16),
        in_specs=[
            pl.BlockSpec((slots, width), lambda s: (0, 0)),
            pl.BlockSpec((1, width, step), lambda s: (0, 0, s)),
            pl.BlockSpec((1, width, step), lambda s: (0, 0, s)),
            pl.BlockSpec((1, step, width), lambda s: (0, s, 0)),
        ],
        out_specs=pl.BlockSpec((slots, width), lambda s: (0, 0)),
        scratch_shapes=[pltpu.VMEM((slots, width), F32)],
        compiler_params=pltpu.CompilerParams(vmem_limit_bytes=48 * MB),
        name="experts",
    )(received, w_gate, w_up, w_down)
    returned = lax.all_to_all(
        reply.reshape(n_expert, capacity, width),
        ("sp", "dp"),
        split_axis=0,
        concat_axis=0,
        tiled=True,
    ).reshape(slots, width)
    return call(combine_body, sds((1, tokens, width), BF16), 4, name="combine")(
        returned, hidden, route_weight, dest_cols
    )


def solution(mesh):
    return jax.shard_map(
        on_device,
        mesh=mesh,
        in_specs=(
            P("dp", "sp", None),
            P("dp", "sp", None),
            P("dp", "sp", None),
            P("dp", "sp", None),
            P("dp", "sp", None),
            P(),
            P(),
            P(),
            P(),
            P("dp", "sp", None),
            P("dp", "sp", None),
            P(("sp", "dp"), None, None),
            P(("sp", "dp"), None, None),
            P(("sp", "dp"), None, None),
        ),
        out_specs=P("dp", "sp", None),
        check_vma=False,
    )
```

profile of v0, /device:TPU:0, one launch (start us, length us, event | category | flops | bytes accessed | tf_op | source)
XLA Modules:
  0.0 175.6 jit_solution(15487832813680247887)
XLA Ops:
  0.0 0.0 copy-start.2
  0.0 0.9 copy.15.ks_ref
  0.9 0.0 copy-start.3
  0.9 0.9 copy-done.3
  1.8 0.0 copy-start.4
  1.8 0.9 copy-done.4
  2.8 0.9 copy-done.5
  3.7 1.1 pack.1
  4.8 7.3 %all-to-all-start = ((bf16[8,400,128]{2,1,0:T(8,128)(2,1)}), bf16[8,400,128]{2,1,0:T(8,128)(2,1)S(1)}, u32[]{:S(2)}, u32[]{:S(2)}) async-start(bf16[8,400,128]{2,1,0:T(8,128)(2,1)} %pack.1), calls=%async_computation | async-start | bytes 1638400 | tf_op jit(solution)/shard_map/all_to_all | solution.py:222
  12.1 0.7 dynamic_slice.3.hs_ref
  12.8 20.2 %all-to-all-done.x_ref = bf16[8,400,128]{2,1,0:T(8,128)(2,1)S(1)} async-done(((bf16[8,400,128]{2,1,0:T(8,128)(2,1)}), bf16[8,400,128]{2,1,0:T(8,128)(2,1)S(1)}, u32[]{:S(2)}, u32[]{:S(2)}) %all-to-all-start) | async-done | bytes 819232 | tf_op jit(solution)/shard_map/all_to_all | solution.py:222
  33.0 7.9 %attention.1 = bf16[8,128,128]{2,1,0:T(8,128)(2,1)} custom-call(f32[2]{0:T(128)S(1)} %dynamic_slice.3.hs_ref, bf16[8,400,128]{2,1,0:T(8,128)(2,1)S(1)} %all-to-all-done.x_ref), custom_call_target="tpu_custom_call" | custom-call | bytes 1048576 | tf_op jit(solution)/shard_map/attention/pallas_call | solution.py:231
  40.9 3.6 %all-to-all-start.1 = ((bf16[8,128,128]{2,1,0:T(8,128)(2,1)}), bf16[8,128,128]{2,1,0:T(8,128)(2,1)S(1)}, u32[]{:S(2)}, u32[]{:S(2)}) async-start(bf16[8,128,128]{2,1,0:T(8,128)(2,1)} %attention.1), calls=%async_computation.1 | async-start | bytes 524288 | tf_op jit(solution)/shard_map/all_to_all | solution.py:239
  44.4 0.0 copy-done.8
  44.4 0.1 copy.16.route_ref
  44.5 0.3 route.1
  44.9 8.6 %all-to-all-done.1.att_ref = bf16[8,128,128]{2,1,0:T(8,128)(2,1)S(1)} async-done(((bf16[8,128,128]{2,1,0:T(8,128)(2,1)}), bf16[8,128,128]{2,1,0:T(8,128)(2,1)S(1)}, u32[]{:S(2)}, u32[]{:S(2)}) %all-to-all-start.1) | async-done | bytes 262176 | tf_op jit(solution)/shard_map/all_to_all | solution.py:239
  53.5 0.0 copy-done.2
  53.5 0.0 copy-done.6
  53.5 0.0 copy-done.7
  53.5 0.0 copy-start.1
  53.5 2.2 %copy-done.1 = bf16[1024,2048]{1,0:T(8,128)(2,1)S(1)} copy-done((bf16[1024,2048]{1,0:T(8,128)(2,1)S(1)}, bf16[1024,2048]{1,0:T(8,128)(2,1)}, u32[]{:S(2)}) %copy-start.1) | copy-done | bytes 4194328
  55.7 1.6 hidden.1
  57.3 52.1 %all_to_all.20 = bf16[32,16,2048]{2,1,0:T(8,128)(2,1)S(1)} all-to-all(bf16[32,16,2048]{2,1,0:T(8,128)(2,1)S(1)} %bitcast.9), channel_id=1, replica_groups=mesh['sp'=8,'dp'=4] {'sp','dp'}, dimensions={0} | all-to-all | bytes 4194304 | tf_op jit(solution)/shard_map/all_to_all | solution.py:246
  109.4 10.9 %experts.1 = bf16[512,2048]{1,0:T(8,128)(2,1)S(1)} custom-call(bf16[512,2048]{1,0:T(8,128)(2,1)S(1)} %bitcast.8, bf16[1,2048,1024]{2,1,0:T(8,128)(2,1)} %wg_ref.1, bf16[1,2048,1024]{2,1,0:T(8,128)(2,1)} %wu_ref.1, bf16[1,1024,2048]{2,1,0:T(8,128)(2,1)} %wd_ref.1), custom_call_target="tpu_custom_call" | custom-call | tf_op jit(solution)/shard_map/experts/pallas_call | solution.py:255
  120.3 0.0 copy-start
  120.3 1.3 copy-done
  121.6 3.7 %all-to-all-start.3 = ((bf16[32,16,2048]{2,1,0:T(8,128)(2,1)}), bf16[32,16,2048]{2,1,0:T(8,128)(2,1)S(1)}, u32[]{:S(2)}, u32[]{:S(2)}) async-start(bf16[32,16,2048]{2,1,0:T(8,128)(2,1)} %bitcast.7), calls=%async_computation.3 | async-start | bytes 4194304 | tf_op jit(solution)/shard_map/all_to_all | solution.py:270
  125.3 0.0 copy-done.9
  125.3 0.1 copy.17.rw_ref
  125.4 48.6 %all-to-all-done.3 = bf16[32,16,2048]{2,1,0:T(8,128)(2,1)S(1)} async-done(((bf16[32,16,2048]{2,1,0:T(8,128)(2,1)}), bf16[32,16,2048]{2,1,0:T(8,128)(2,1)S(1)}, u32[]{:S(2)}, u32[]{:S(2)}) %all-to-all-start.3) | async-done | bytes 2097184 | tf_op jit(solution)/shard_map/all_to_all | solution.py:270
  174.0 1.6 combine.1
  (5 shorter events, 0.0 us)
Async XLA Ops:
  0.0 53.5 %copy-start.2 = (bf16[1,128,2048]{2,1,0:T(8,128)(2,1)S(1)}, bf16[1,128,2048]{2,1,0:T(8,128)(2,1)}, u32[]{:S(2)}) copy-start(bf16[1,128,2048]{2,1,0:T(8,128)(2,1)} %stream_ref.1) | copy-start | bytes 1572868
  0.9 1.0 copy-start.3
  1.8 0.9 copy-start.4
  2.8 0.9 copy-start.5
  3.7 40.7 %copy-start.8 = (s32[1,128,2]{1,2,0:T(2,128)S(1)}, s32[1,128,2]{1,2,0:T(2,128)}, u32[]{:S(2)}) copy-start(s32[1,128,2]{1,2,0:T(2,128)} %param.23) | copy-start | bytes 3076
  3.7 49.8 %copy-start.6 = (f32[2048]{0:T(1024)S(1)}, f32[2048]{0:T(1024)}, u32[]{:S(2)}) copy-start(f32[2048]{0:T(1024)} %param.22) | copy-start | bytes 24580
  3.7 49.8 %copy-start.7 = (f32[1024]{0:T(1024)S(1)}, f32[1024]{0:T(1024)}, u32[]{:S(2)}) copy-start(f32[1024]{0:T(1024)} %param.20) | copy-start | bytes 12292
  4.8 28.2 %all-to-all-start = ((bf16[8,400,128]{2,1,0:T(8,128)(2,1)}), bf16[8,400,128]{2,1,0:T(8,128)(2,1)S(1)}, u32[]{:S(2)}, u32[]{:S(2)}) async-start(bf16[8,400,128]{2,1,0:T(8,128)(2,1)} %pack.1), calls=%async_computation | async-start | bytes 1638400 | tf_op jit(solution)/shard_map/all_to_all | solution.py:222
  40.9 12.7 %all-to-all-start.1 = ((bf16[8,128,128]{2,1,0:T(8,128)(2,1)}), bf16[8,128,128]{2,1,0:T(8,128)(2,1)S(1)}, u32[]{:S(2)}, u32[]{:S(2)}) async-start(bf16[8,128,128]{2,1,0:T(8,128)(2,1)} %attention.1), calls=%async_computation.1 | async-start | bytes 524288 | tf_op jit(solution)/shard_map/all_to_all | solution.py:239
  53.5 2.2 %copy-start.1 = (bf16[1024,2048]{1,0:T(8,128)(2,1)S(1)}, bf16[1024,2048]{1,0:T(8,128)(2,1)}, u32[]{:S(2)}) copy-start(bf16[1024,2048]{1,0:T(8,128)(2,1)} %w_ref.1) | copy-start | bytes 12582916
  120.3 1.3 copy-start
  121.6 3.7 %copy-start.9 = (f32[1,128,2]{1,2,0:T(2,128)S(1)}, f32[1,128,2]{1,2,0:T(2,128)}, u32[]{:S(2)}) copy-start(f32[1,128,2]{1,2,0:T(2,128)} %param.24) | copy-start | bytes 3076
  121.6 52.4 %all-to-all-start.3 = ((bf16[32,16,2048]{2,1,0:T(8,128)(2,1)}), bf16[32,16,2048]{2,1,0:T(8,128)(2,1)S(1)}, u32[]{:S(2)}, u32[]{:S(2)}) async-start(bf16[32,16,2048]{2,1,0:T(8,128)(2,1)} %bitcast.7), calls=%async_computation.3 | async-start | bytes 4194304 | tf_op jit(solution)/shard_map/all_to_all | solution.py:270
where the time goes:
time: 176 us
  waiting for transfers between devices  77.4 us (44%)
  blocking collectives  52.1 us (30%)
  Pallas kernels  23.3 us (13%)
  starting transfers between devices  14.5 us (8%)
  local copies, waits for them, and re-layouts  8.2 us (5%)
    all_to_all x1, blocking collectives, on_device(): lax.all_to_all(send.reshape(n_expert, capacity, width), ('sp', 'dp'), spl...  52.1 us
    all_to_all x1, waiting for transfers between devices, on_device(): lax.all_to_all(reply.reshape(n_expert, capacity, width), ('sp', 'dp'), sp...  48.6 us
    all_to_all x1, waiting for transfers between devices, on_device(): got = lax.all_to_all(sent, 'sp', split_axis=0, concat_axis=0, tiled=True)  20.2 us
    pallas_call x1, Pallas kernels, on_device(): pl.pallas_call(expert_body, grid=(f // step,), out_shape=sds((slots, widt...  10.9 us
    all_to_all x1, waiting for transfers between devices, on_device(): att = lax.all_to_all(att, 'sp', split_axis=0, concat_axis=0, tiled=True)  8.62 us
    pallas_call x1, Pallas kernels, on_device(): call(attention_body, sds((size_sp, tokens, cols), BF16), 2, in_specs=[SM,...  7.89 us
    unnamed x23, local copies, waits for them, and re-layouts  7.47 us
    all_to_all x1, starting transfers between devices, on_device(): got = lax.all_to_all(sent, 'sp', split_axis=0, concat_axis=0, tiled=True)  7.31 us
  transfers between devices with their start and end apart: 3, of which 3 were waited for; matrix products, arithmetic and copies ran while one was open for 1% of the time, Pallas kernels for 0%

commit v1 on v0

v1 whole, which is shorter than its diff:
```python
import functools
import math

import jax
import jax.numpy as jnp
from jax import lax
from jax.experimental import pallas as pl
from jax.experimental.pallas import tpu as pltpu
from jax.sharding import PartitionSpec as P


HD = 64
GROUPS = 4
CORES = 2
CHUNKS = ((2,), (3,), (0, 1))
norm_eps = 1e-05
F32 = jnp.float32
BF16 = jnp.bfloat16
MB = 1024 * 1024
FLOPS = 1.5e7
BYTES = 3.0e6

VM = pl.BlockSpec(memory_space=pltpu.VMEM)
SM = pl.BlockSpec(memory_space=pltpu.SMEM)
NT = (((1,), (1,)), ((), ()))


def call(body, out, n_in, scratch=(), limit=8, in_specs=None, us=1.0):
    return pl.pallas_call(
        body,
        out_shape=out,
        in_specs=in_specs or [VM] * n_in,
        out_specs=jax.tree.map(lambda _: VM, out),
        scratch_shapes=list(scratch),
        compiler_params=pltpu.CompilerParams(vmem_limit_bytes=limit * MB),
        cost_estimate=pl.CostEstimate(flops=int(us * FLOPS), bytes_accessed=int(us * BYTES), transcendentals=0),
    )


def iota(shape, dim):
    return lax.broadcasted_iota(jnp.int32, shape, dim)


def pack_body(q_ref, k_ref, v_ref, ks_ref, out_ref):
    n, rows, cols = out_ref.shape
    tokens, heads = ks_ref.shape[1], ks_ref.shape[2]
    local = heads // n
    pieces = tokens // cols
    eye = (iota((heads, heads), 0) == iota((heads, heads), 1)).astype(BF16)
    shift = lax.dot_general(eye, ks_ref[0], NT, preferred_element_type=F32)
    pad = rows - 3 * tokens
    for d in range(n):
        lanes = slice(d * cols, (d + 1) * cols)
        out_ref[d, 0:tokens, :] = q_ref[0, :, lanes]
        out_ref[d, tokens : 2 * tokens, :] = k_ref[0, :, lanes]
        out_ref[d, 2 * tokens : 3 * tokens, :] = v_ref[0, :, lanes]
        tail = [
            shift[d * local + h : d * local + h + 1, p * cols : (p + 1) * cols]
            for h in range(local)
            for p in range(pieces)
        ]
        tail.append(jnp.zeros((pad - len(tail), cols), F32))
        out_ref[d, 3 * tokens :, :] = jnp.concatenate(tail, axis=0).astype(BF16)


def pick_body(me_ref, q_ref, k_ref, v_ref, ks_ref, *out_refs):
    rows, cols = out_refs[0].shape
    tokens, heads = ks_ref.shape[1], ks_ref.shape[2]
    local = heads // len(out_refs)
    pad = rows - 3 * tokens
    line, head = iota((pad, heads), 0), iota((pad, heads), 1)
    for k, out_ref in enumerate(out_refs):
        target = me_ref[1] ^ k
        lanes = pl.ds(pl.multiple_of(target * cols, cols), cols)
        out_ref[0:tokens, :] = q_ref[0, :, lanes]
        out_ref[tokens : 2 * tokens, :] = k_ref[0, :, lanes]
        out_ref[2 * tokens : 3 * tokens, :] = v_ref[0, :, lanes]
        take = ((head == line + target * local) & (line < local)).astype(F32).astype(BF16)
        out_ref[3 * tokens :, :] = lax.dot_general(
            take, ks_ref[0], NT, preferred_element_type=F32
        ).astype(BF16)


def attention_body(me_ref, hs_ref, *refs, fetches):
    n = (len(refs) - 5 - 2 * fetches)
    x_refs, refs = refs[:n], refs[n:]
    sources, (out_ref, *kept), (x_ref, z_ref, w_ref, sems) = (
        refs[:fetches],
        refs[fetches : 2 * fetches + 1],
        refs[2 * fetches + 1 :],
    )
    copies = [
        pltpu.make_async_copy(source, target, sems.at[i])
        for i, (source, target) in enumerate(zip(sources, kept))
    ]
    for copy in copies:
        copy.start()
    for k, ref in enumerate(x_refs):
        x_ref[me_ref[1] ^ k] = ref[...]
    n, _, cols = x_ref.shape
    tokens = out_ref.shape[1]
    local = cols // HD
    pieces = tokens // cols
    lane = iota((tokens, cols), 1) // HD
    keys = x_ref[:, tokens : 2 * tokens, :].reshape(n * tokens, cols)
    values = x_ref[:, 2 * tokens : 3 * tokens, :].reshape(n * tokens, cols)
    row, col = iota((2 * tokens, 2 * tokens), 0), iota((2 * tokens, 2 * tokens), 1)
    summing = jnp.where((col >= tokens) | (row % tokens >= col), 1.0, 0.0).astype(BF16)
    causal = iota((tokens, tokens), 1) < iota((tokens, tokens), 0)
    for i in range(n):
        total = None
        for h in range(local):
            q = x_ref[i, 0:tokens, :].astype(F32) * (1.0 / math.sqrt(HD))
            q = jnp.where(lane == h, q, 0.0).astype(BF16)
            span = (i + 1) * tokens
            z_ref[h, :, 0:span] = lax.dot_general(
                q, keys[0:span], NT, preferred_element_type=F32
            )
            carry = None
            for j in range(i, -1, -1):
                at = slice(j * tokens, (j + 1) * tokens)
                base = 3 * tokens + h * pieces
                off = [x_ref[j, base + p : base + p + 1, :] for p in range(pieces)]
                off = off[0] if pieces == 1 else jnp.concatenate(off, axis=1)
                z = z_ref[h, :, at] + (off.astype(F32) + hs_ref[me_ref[1] * local + h])
                breaks = -(jnp.maximum(z, 0.0) + jnp.log(1.0 + jnp.exp(-jnp.abs(z))))
                if j == i:
                    breaks = jnp.where(causal, breaks, 0.0)
                high = breaks.astype(BF16)
                low = (breaks - high.astype(F32)).astype(BF16)
                sums = jnp.dot(
                    jnp.concatenate([high, low], axis=1), summing, preferred_element_type=F32
                )
                power = z + sums[:, 0:tokens]
                if carry is not None:
                    power = power + carry
                weight = jnp.exp(power)
                if j == i:
                    weight = jnp.where(causal, weight, 0.0)
                w_ref[h, :, at] = weight.astype(BF16)
                part = sums[:, tokens:]
                carry = part if carry is None else carry + part
            got = jnp.dot(w_ref[h, :, 0:span], values[0:span], preferred_element_type=F32)
            total = got if total is None else jnp.where(lane == h, got, total)
        out_ref[i] = total.astype(BF16)
    for copy in copies:
        copy.wait()


def route_body(me_ref, route_ref, rw_ref, row_ref, col_ref, *meta_refs, plane, cap):
    tokens = route_ref.shape[1]
    bits = plane.bit_length() - 1
    zme, pme = me_ref[0] >> bits, me_ref[0] & (plane - 1)
    ids = route_ref[0].astype(F32)
    eye = iota((tokens, tokens), 0) == iota((tokens, tokens), 1)
    before = (iota((tokens, tokens), 0) < iota((tokens, tokens), 1)).astype(BF16)

    def to_row(col):
        return jnp.sum(jnp.where(eye, col, 0.0), axis=0, keepdims=True)

    def to_col(row):
        return jnp.sum(jnp.where(eye, row, 0.0), axis=1, keepdims=True)

    def count(hot):
        return jnp.dot(hot.astype(BF16), before, preferred_element_type=F32)

    e_rows = [to_row(ids[:, k : k + 1]) for k in range(2)]
    names = iota((GROUPS * plane, tokens), 0).astype(F32)
    hot = [(names == e).astype(F32) for e in e_rows]
    earlier = count(hot[0] + hot[1])
    ranks = [jnp.sum(h * earlier, axis=0, keepdims=True) for h in hot]
    group = e_rows[0].astype(jnp.int32) >> bits
    in_group = (iota((8, tokens), 0) == group).astype(F32)
    place = jnp.sum(in_group * count(in_group), axis=0, keepdims=True)
    spot = [e.astype(jnp.int32) & (plane - 1) for e in e_rows]
    rows = [jnp.where(group == (zme ^ d), place, -1.0) for d in range(GROUPS)]
    row_ref[...] = jnp.concatenate(rows + [jnp.zeros((4, tokens), F32)], axis=0).astype(jnp.int32)
    lane = iota((tokens, 128), 1)
    cols = [to_col(r) for r in rows]
    table = jnp.zeros((tokens, 128), F32)
    for k, c in enumerate(cols):
        table = jnp.where(lane == k, c, table)
    col_ref[...] = table.astype(jnp.int32)
    offset = [(p ^ pme) for p in spot]
    slot = iota((tokens, tokens), 1).astype(F32)
    for d, (c, ref) in enumerate(zip(cols, meta_refs)):
        chunk = next(chunk for chunk in CHUNKS if d in chunk)
        sources, source = len(chunk), chunk.index(d)
        relay = [
            to_col(((q * sources + source) * cap).astype(F32) + r) for q, r in zip(offset, ranks)
        ]
        pick = slot == c
        out = [
            jnp.sum(jnp.where(pick, v + 1.0, 0.0), axis=0, keepdims=True) - 1.0 for v in relay
        ]
        out += [
            jnp.sum(jnp.where(pick, rw_ref[0, :, k : k + 1], 0.0), axis=0, keepdims=True)
            for k in range(2)
        ]
        ref[...] = jnp.concatenate(out + [jnp.zeros((4, tokens), F32)], axis=0)


def hidden_body(att_ref, stream_ref, mg_ref, w_ref, pg_ref, dest_ref, hid_ref, *far_refs):
    n, tokens, cols = att_ref.shape
    pieces = [att_ref[s].astype(F32) for s in range(n)]
    if cols % 128 == 0:
        pieces = [jnp.concatenate(pieces, axis=1)]
    size = pieces[0].shape[1]
    square = sum(jnp.sum(p * p, axis=1, keepdims=True) for p in pieces)
    scale = lax.rsqrt(square / (n * cols) + norm_eps)
    mixed = None
    for s, p in enumerate(pieces):
        at = slice(s * size, (s + 1) * size)
        normed = (p * scale * mg_ref[:, at]).astype(BF16)
        part = jnp.dot(normed, w_ref[at, :], preferred_element_type=F32)
        mixed = part if mixed is None else mixed + part
    summed = stream_ref[0].astype(F32) + mixed
    mean = jnp.mean(summed * summed, axis=1, keepdims=True)
    hidden = (summed * lax.rsqrt(mean + norm_eps) * pg_ref[...]).astype(BF16)
    hid_ref[...] = hidden
    for d, ref in enumerate(far_refs):
        pick = iota((ref.shape[0], tokens), 0) == dest_ref[d : d + 1, :]
        ref[...] = jnp.dot(
            pick.astype(F32).astype(BF16), hidden, preferred_element_type=F32
        ).astype(BF16)


def relay_body(*refs, sources):
    x_refs, meta_refs, out_refs = refs[:sources], refs[sources : 2 * sources], refs[2 * sources :]
    half = x_refs[0].shape[0]
    block = out_refs[0].shape[0]
    slot = iota((block * len(out_refs), half), 0)
    rows = None
    for x_ref, meta_ref in zip(x_refs, meta_refs):
        place = meta_ref[0:2, 0:half].astype(jnp.int32)
        pick = (slot == place[0:1]) | (slot == place[1:2])
        part = jnp.dot(pick.astype(F32).astype(BF16), x_ref[...], preferred_element_type=F32)
        rows = part if rows is None else rows + part
    rows = rows.astype(BF16)
    for m, ref in enumerate(out_refs):
        ref[...] = rows[m * block : (m + 1) * block]


def expert_body(*refs, takes):
    x_refs, (wg_ref, wu_ref, wd_ref), out_refs = (
        refs[: len(takes)],
        refs[len(takes) : len(takes) + 3],
        refs[len(takes) + 3 :],
    )
    parts = [ref[0:take] for ref, take in zip(x_refs, takes)]
    x = parts[0] if len(parts) == 1 else jnp.concatenate(parts, axis=0)
    gate = jnp.dot(x, wg_ref[0], preferred_element_type=F32)
    upper = jnp.dot(x, wu_ref[0], preferred_element_type=F32)
    inner = (gate / (1.0 + jnp.exp(-gate)) * upper).astype(BF16)
    out = jnp.dot(inner, wd_ref[0], preferred_element_type=F32).astype(BF16)
    at = 0
    for ref in out_refs:
        ref[...] = out[at : at + ref.shape[0]]
        at += ref.shape[0]


def second_halves_body(*refs):
    out_ref = refs[-1]
    part = out_ref.shape[0] // (len(refs) - 1)
    for m, ref in enumerate(refs[:-1]):
        out_ref[m * part : (m + 1) * part] = ref[part:]


def join_body(own_ref, back_ref, *out_refs):
    part = out_refs[0].shape[0] // 2
    for m, ref in enumerate(out_refs):
        at = slice(m * part, (m + 1) * part)
        ref[0:part] = own_ref[at]
        ref[part:] = back_ref[at]


def gather_body(*refs, sources):
    meta_refs, row_refs, out_refs = refs[:sources], refs[sources:-sources], refs[-sources:]
    parts = [ref[...] for ref in row_refs]
    rows = parts[0] if len(parts) == 1 else jnp.concatenate(parts, axis=0)
    for meta_ref, out_ref in zip(meta_refs, out_refs):
        half = out_ref.shape[0]
        eye = iota((half, half), 0) == iota((half, half), 1)
        slot = iota((half, rows.shape[0]), 1).astype(F32)
        total = None
        for k in range(2):
            place, weight = [
                jnp.sum(jnp.where(eye, meta_ref[r : r + 1, 0:half], 0.0), axis=1, keepdims=True)
                for r in (k, 2 + k)
            ]
            pick = (slot == place).astype(F32).astype(BF16)
            part = jnp.dot(pick, rows, preferred_element_type=F32) * weight
            total = part if total is None else total + part
        out_ref[...] = total.astype(BF16)


def combine_body(*refs):
    far_refs, (hid_ref, dest_ref, out_ref) = refs[:-3], refs[-3:]
    tokens = hid_ref.shape[0]
    result = hid_ref[...].astype(F32)
    for d, ref in enumerate(far_refs):
        slot = iota((tokens, ref.shape[0]), 1)
        hot = (slot == dest_ref[:, d : d + 1]).astype(F32).astype(BF16)
        result = result + jnp.dot(hot, ref[...], preferred_element_type=F32)
    out_ref[0] = result.astype(BF16)


def on_device(
    stream,
    queries,
    keys_in,
    values_in,
    key_shift,
    head_shift,
    mix_gain,
    out_weight,
    post_gain,
    route,
    route_weight,
    w_gate,
    w_up,
    w_down,
):
    tokens, width = stream.shape[1], stream.shape[2]
    size_sp, size_dp = lax.axis_size("sp"), lax.axis_size("dp")
    heads = key_shift.shape[2]
    local = heads // size_sp
    cols = queries.shape[2] // size_sp
    rows = 3 * tokens + 16
    n_expert = size_sp * size_dp
    plane = n_expert // GROUPS
    chips = plane // CORES
    cap = tokens // plane
    half = tokens // 2
    both = ("sp", "dp")
    sds = jax.ShapeDtypeStruct
    sp = lax.axis_index("sp")
    me = jnp.stack([sp * size_dp + lax.axis_index("dp"), sp]).astype(jnp.int32)

    def swap(array, bit):
        return lax.ppermute(array, both, [(i, i ^ bit) for i in range(n_expert)])

    if cols == tokens:
        sent = call(
            pick_body, (sds((rows, cols), BF16),) * size_sp, 5, in_specs=[SM, VM, VM, VM, VM]
        )(me, queries, keys_in, values_in, key_shift)
    else:
        sent = call(pack_body, sds((size_sp, rows, cols), BF16), 4)(
            queries, keys_in, values_in, key_shift
        )
        sent = [
            lax.dynamic_index_in_dim(sent, sp ^ k, 0, keepdims=False) for k in range(size_sp)
        ]
    got = [sent[0]] + [None] * (size_sp - 1)
    for k in range(size_sp - 1, 0, -1):
        got[k] = swap(sent[k], k * size_dp)
    dest_rows, dest_cols, *metas = call(
        functools.partial(route_body, plane=plane, cap=cap),
        (sds((8, tokens), jnp.int32), sds((tokens, 128), jnp.int32))
        + (sds((8, tokens), F32),) * GROUPS,
        3,
        in_specs=[SM, VM, VM],
    )(me, route, route_weight)
    metas = [metas[0]] + [swap(metas[d], d * plane) for d in range(1, GROUPS)]
    got, metas = lax.optimization_barrier((got, metas))
    seq = size_sp * tokens
    later = [
        pltpu.with_memory_space_constraint(array, pltpu.HBM)
        for array in (out_weight, stream, mix_gain[None], post_gain[None], w_down)
    ]
    att, out_weight, stream, mix_gain, post_gain, w_down = call(
        functools.partial(attention_body, fetches=len(later)),
        (sds((size_sp, tokens, cols), BF16),) + tuple(sds(x.shape, x.dtype) for x in later),
        0,
        in_specs=[SM, SM]
        + [VM] * size_sp
        + [pl.BlockSpec(memory_space=pltpu.HBM)] * len(later),
        scratch=[
            pltpu.VMEM((size_sp, rows, cols), BF16),
            pltpu.VMEM((local, tokens, seq), F32),
            pltpu.VMEM((local, tokens, seq), BF16),
            pltpu.SemaphoreType.DMA((len(later),)),
        ],
        us=8,
    )(me, head_shift, *got, *later)
    att = lax.all_to_all(att, "sp", split_axis=0, concat_axis=0, tiled=True)
    row = lambda count: sds((count, width), BF16)
    hidden, *far = call(
        hidden_body, (row(tokens),) + (row(half),) * GROUPS, 6, us=2
    )(att, stream, mix_gain, out_weight, post_gain, dest_rows)
    for d in range(1, GROUPS):
        far[d] = swap(far[d], d * plane)

    def experts(pieces, takes, outs):
        if any(take % 8 for take in takes):
            pieces = [jnp.concatenate([p[:t] for p, t in zip(pieces, takes)], axis=0)]
            takes = [sum(takes)]
        return call(
            functools.partial(expert_body, takes=takes),
            tuple(row(o) for o in outs),
            len(takes) + 3,
            limit=8,
            us=0.02 * sum(takes),
        )(*pieces, w_gate, w_up, w_down)

    sums = [None] * GROUPS
    for chunk in CHUNKS:
        sources = len(chunk)
        block = row(CORES * cap * sources)
        part = cap * sources
        blocks = call(
            functools.partial(relay_body, sources=sources), (block,) * chips, 2 * sources
        )(*[far[d] for d in chunk], *[metas[d] for d in chunk])
        held = [blocks[0]] + [swap(blocks[m], CORES * m) for m in range(1, chips)]
        if part % 16:
            other = jnp.concatenate([b[part:] for b in held], axis=0)
        else:
            other = call(second_halves_body, row(chips * part), chips)(*held)
        other = swap(other, 1)
        own, reply = experts(
            held + [other], [part] * chips + [chips * part], [chips * part, chips * part]
        )
        back = swap(reply, 1)
        if part % 16:
            joined = [
                jnp.concatenate([a[m * part : (m + 1) * part] for a in (own, back)], axis=0)
                for m in range(chips)
            ]
        else:
            joined = call(join_body, (block,) * chips, 2)(own, back)
        got_back = [joined[0]] + [swap(joined[m], CORES * m) for m in range(1, chips)]
        if block.shape[0] % 16:
            got_back = [jnp.concatenate(got_back, axis=0)]
        got_back = call(
            functools.partial(gather_body, sources=sources),
            (row(half),) * sources,
            sources + len(got_back),
        )(*[metas[d] for d in chunk], *got_back)
        for d, total in zip(chunk, got_back):
            sums[d] = swap(total, d * plane) if d else total
    return call(combine_body, sds((1, tokens, width), BF16), GROUPS + 2)(*sums, hidden, dest_cols)


def solution(mesh):
    return jax.shard_map(
        on_device,
        mesh=mesh,
        in_specs=(
            P("dp", "sp", None),
            P("dp", "sp", None),
            P("dp", "sp", None),
            P("dp", "sp", None),
            P("dp", "sp", None),
            P(),
            P(),
            P(),
            P(),
            P("dp", "sp", None),
            P("dp", "sp", None),
            P(("sp", "dp"), None, None),
            P(("sp", "dp"), None, None),
            P(("sp", "dp"), None, None),
        ),
        out_specs=P("dp", "sp", None),
        check_vma=False,
    )
```

time: 176 us -> 154 us (0.88)
  blocking collectives: 52.1 us -> 15.2 us
  starting transfers between devices: 14.5 us -> 46.7 us
  waiting for transfers between devices: 77.4 us -> 60 us
  local copies, waits for them, and re-layouts: 8.2 us -> 5.88 us
  Pallas kernels: 23.3 us -> 25.2 us
    all_to_all x3 -> x0, waiting for transfers between devices: 77.4 us -> none  [the longest x1 48.6 us: on_device(): lax.all_to_all(reply.reshape(n_expert, capacity, width), ('sp', 'dp'), sp...]
    ppermute x0 -> x40, waiting for transfers between devices: none -> 60 us  [swap(): return lax.ppermute(array, both, [(i, i ^ bit) for i in range(n_expert)])]
    ppermute x0 -> x40, starting transfers between devices: none -> 46.7 us  [swap(): return lax.ppermute(array, both, [(i, i ^ bit) for i in range(n_expert)])]
    all_to_all x1, blocking collectives: 52.1 us -> 15.2 us  [on_device(): att = lax.all_to_all(att, 'sp', split_axis=0, concat_axis=0, tiled=True)]
    all_to_all x3 -> x0, starting transfers between devices: 14.5 us -> none  [the longest x1 7.31 us: on_device(): got = lax.all_to_all(sent, 'sp', split_axis=0, concat_axis=0, tiled=True)]
    pallas_call x6 -> x20, Pallas kernels: 23.3 us -> 25.2 us  [the longest x1 9.99 us: on_device(): call(functools.partial(attention_body, fetches=len(later)), (sds((size_sp...]
    unnamed x23 -> x15, local copies, waits for them, and re-layouts: 7.47 us -> 5.88 us
  transfers between devices with their start and end apart: 3 -> 40, of which waited for: 3 -> 17; matrix products, arithmetic and copies ran while one was open for 1% -> 1% of each run, Pallas kernels for 0% -> 7%
where the time goes in v1:
time: 154 us; the launch traced here: 153 us
  waiting for transfers between devices  60 us (39%)
  starting transfers between devices  46.7 us (30%)
  Pallas kernels  25.2 us (16%)
  blocking collectives  15.2 us (10%)
  local copies, waits for them, and re-layouts  5.88 us (4%)
    ppermute x40, waiting for transfers between devices, swap(): return lax.ppermute(array, both, [(i, i ^ bit) for i in range(n_expert)])  60 us
    ppermute x40, starting transfers between devices, swap(): return lax.ppermute(array, both, [(i, i ^ bit) for i in range(n_expert)])  46.7 us
    all_to_all x1, blocking collectives, on_device(): att = lax.all_to_all(att, 'sp', split_axis=0, concat_axis=0, tiled=True)  15.2 us
    pallas_call x1, Pallas kernels, on_device(): call(functools.partial(attention_body, fetches=len(later)), (sds((size_sp...  9.99 us
    pallas_call x3, Pallas kernels, experts(): call(functools.partial(expert_body, takes=takes), tuple((row(o) for o in...  7.14 us
    unnamed x15, local copies, waits for them, and re-layouts  5.88 us
  transfers between devices with their start and end apart: 40, of which 17 were waited for; matrix products, arithmetic and copies ran while one was open for 1% of the time, Pallas kernels for 7%

profile of v1, /device:TPU:0, one launch (start us, length us, event | category | flops | bytes accessed | tf_op | source)
XLA Modules:
  0.0 153.3 jit_solution(17440380816796006207)
XLA Ops:
  4.6 3.0 %collective-permute-start = (bf16[400,128]{1,0:T(8,128)(2,1)S(1)}, bf16[400,128]{1,0:T(8,128)(2,1)S(1)}, u32[]{:S(2)}, u32[]{:S(2)}) collective-permute-start(bf16[400,128]{1,0:T(8,128)(2,1)S(1)} %get-tuple-element.75), channel_id=1, source_target_pairs={{0,4},{1,5},{2,6},{3,7},{4,0},{5,1},{6,2},{7,3},{8,12},{9,13},{10,... | collective-permute-start | bytes 307208 | tf_op jit(solution)/shard_map/ppermute | solution.py:341
  7.6 1.6 %collective-permute-start.1 = (bf16[400,128]{1,0:T(8,128)(2,1)S(1)}, bf16[400,128]{1,0:T(8,128)(2,1)S(1)}, u32[]{:S(2)}, u32[]{:S(2)}) collective-permute-start(bf16[400,128]{1,0:T(8,128)(2,1)S(1)} %get-tuple-element.76), channel_id=1, source_target_pairs={{0,8},{1,9},{2,10},{3,11},{4,12},{5,13},{6,14},{7,15},{8,0},{9,1},... | collective-permute-start | bytes 307208 | tf_op jit(solution)/shard_map/ppermute | solution.py:341
  12.5 2.6 %collective-permute-start.8 = (f32[8,128]{1,0:T(8,128)S(1)}, f32[8,128]{1,0:T(8,128)S(1)}, u32[]{:S(2)}, u32[]{:S(2)}) collective-permute-start(f32[8,128]{1,0:T(8,128)S(1)} %get-tuple-element.84), channel_id=1, source_target_pairs={{0,16},{1,17},{2,18},{3,19},{4,20},{5,21},{6,22},{7,23},{8,24},{9,... | collective-permute-start | bytes 12296 | tf_op jit(solution)/shard_map/ppermute | solution.py:341
  17.0 2.6 %collective-permute-start.3 = (bf16[400,128]{1,0:T(8,128)(2,1)S(1)}, bf16[400,128]{1,0:T(8,128)(2,1)S(1)}, u32[]{:S(2)}, u32[]{:S(2)}) collective-permute-start(bf16[400,128]{1,0:T(8,128)(2,1)S(1)} %get-tuple-element.78), channel_id=1, source_target_pairs={{0,16},{1,17},{2,18},{3,19},{4,20},{5,21},{6,22},{7,23},{8,24},{9,... | collective-permute-start | bytes 307208 | tf_op jit(solution)/shard_map/ppermute | solution.py:341
  20.6 2.9 %collective-permute-start.5 = (bf16[400,128]{1,0:T(8,128)(2,1)S(1)}, bf16[400,128]{1,0:T(8,128)(2,1)S(1)}, u32[]{:S(2)}, u32[]{:S(2)}) collective-permute-start(bf16[400,128]{1,0:T(8,128)(2,1)S(1)} %get-tuple-element.80), channel_id=1, source_target_pairs={{0,24},{1,25},{2,26},{3,27},{4,28},{5,29},{6,30},{7,31},{8,16},{9,... | collective-permute-start | bytes 307208 | tf_op jit(solution)/shard_map/ppermute | solution.py:341
  24.6 5.3 %collective-permute-done.3.refs_4_ = bf16[400,128]{1,0:T(8,128)(2,1)S(1)} collective-permute-done((bf16[400,128]{1,0:T(8,128)(2,1)S(1)}, bf16[400,128]{1,0:T(8,128)(2,1)S(1)}, u32[]{:S(2)}, u32[]{:S(2)}) %collective-permute-start.3) | collective-permute-done | bytes 102432 | tf_op jit(solution)/shard_map/ppermute | solution.py:341
  29.9 3.6 %collective-permute-done.4.refs_5_ = bf16[400,128]{1,0:T(8,128)(2,1)S(1)} collective-permute-done((bf16[400,128]{1,0:T(8,128)(2,1)S(1)}, bf16[400,128]{1,0:T(8,128)(2,1)S(1)}, u32[]{:S(2)}, u32[]{:S(2)}) %collective-permute-start.4) | collective-permute-done | bytes 102432 | tf_op jit(solution)/shard_map/ppermute | solution.py:341
  34.2 10.0 %shard_map.138 = (bf16[8,128,128]{2,1,0:T(8,128)(2,1)S(1)}, bf16[1024,2048]{1,0:T(8,128)(2,1)S(1)}, bf16[1,128,2048]{2,1,0:T(8,128)(2,1)S(1)}, f32[1,1024]{1,0:T...) custom-call(s32[2]{0:T(128)S(1)} %pad_add_fusion.me_ref, f32[16]{0:T(128)S(1)} %copy-done.5, ...), custom_call_target="tpu_custom_call" | custom-call | flops 120000000 | bytes 24000000 | tf_op jit(solution)/shard_map/pallas_call | solution.py:371
  44.2 15.2 %all_to_all.5.att_ref = bf16[8,128,128]{2,1,0:T(8,128)(2,1)S(1)} all-to-all(bf16[8,128,128]{2,1,0:T(8,128)(2,1)S(1)} %get-tuple-element.96), channel_id=1, replica_groups=mesh['sp'=8,'dp'=4] {'sp'}, dimensions={0} | all-to-all | bytes 524288 | tf_op jit(solution)/shard_map/all_to_all | solution.py:386
  59.4 1.4 shard_map.139
  60.9 6.4 %collective-permute-done.10.refs_1_ = bf16[64,2048]{1,0:T(8,128)(2,1)S(1)} collective-permute-done((bf16[64,2048]{1,0:T(8,128)(2,1)S(1)}, bf16[64,2048]{1,0:T(8,128)(2,1)S(1)}, u32[]{:S(2)}, u32[]{:S(2)}) %collective-permute-start.10) | collective-permute-done | bytes 262176 | tf_op jit(solution)/shard_map/ppermute | solution.py:341
  67.9 1.6 %collective-permute-start.11 = (bf16[64,2048]{1,0:T(8,128)(2,1)S(1)}, bf16[64,2048]{1,0:T(8,128)(2,1)S(1)}, u32[]{:S(2)}, u32[]{:S(2)}) collective-permute-start(bf16[64,2048]{1,0:T(8,128)(2,1)S(1)} %get-tuple-element.105), channel_id=1, source_target_pairs={{0,2},{1,3},{2,0},{3,1},{4,6},{5,7},{6,4},{7,5},{8,10},{9,11},{10,... | collective-permute-start | bytes 786440 | tf_op jit(solution)/shard_map/ppermute | solution.py:341
  72.1 3.0 %collective-permute-done.11.refs_1_ = bf16[64,2048]{1,0:T(8,128)(2,1)S(1)} collective-permute-done((bf16[64,2048]{1,0:T(8,128)(2,1)S(1)}, bf16[64,2048]{1,0:T(8,128)(2,1)S(1)}, u32[]{:S(2)}, u32[]{:S(2)}) %collective-permute-start.11) | collective-permute-done | bytes 262176 | tf_op jit(solution)/shard_map/ppermute | solution.py:341
  75.0 4.0 %collective-permute-done.12.refs_2_ = bf16[64,2048]{1,0:T(8,128)(2,1)S(1)} collective-permute-done((bf16[64,2048]{1,0:T(8,128)(2,1)S(1)}, bf16[64,2048]{1,0:T(8,128)(2,1)S(1)}, u32[]{:S(2)}, u32[]{:S(2)}) %collective-permute-start.12) | collective-permute-done | bytes 262176 | tf_op jit(solution)/shard_map/ppermute | solution.py:341
  79.2 1.8 %collective-permute-start.30 = (bf16[64,2048]{1,0:T(8,128)(2,1)S(1)}, bf16[64,2048]{1,0:T(8,128)(2,1)S(1)}, u32[]{:S(2)}, u32[]{:S(2)}) collective-permute-start(bf16[64,2048]{1,0:T(8,128)(2,1)S(1)} %get-tuple-element.130), channel_id=1, source_target_pairs={{0,24},{1,25},{2,26},{3,27},{4,28},{5,29},{6,30},{7,31},{8,16},{9,... | collective-permute-start | bytes 786440 | tf_op jit(solution)/shard_map/ppermute | solution.py:341
  81.4 1.6 %collective-permute-start.21 = (bf16[32,2048]{1,0:T(8,128)(2,1)S(1)}, bf16[32,2048]{1,0:T(8,128)(2,1)S(1)}, u32[]{:S(2)}, u32[]{:S(2)}) collective-permute-start(bf16[32,2048]{1,0:T(8,128)(2,1)S(1)} %get-tuple-element.120), channel_id=1, source_target_pairs={{0,2},{1,3},{2,0},{3,1},{4,6},{5,7},{6,4},{7,5},{8,10},{9,11},{10,... | collective-permute-start | bytes 393224 | tf_op jit(solution)/shard_map/ppermute | solution.py:341
  83.0 1.4 collective-permute-start.22
  85.0 4.8 %collective-permute-done.30.refs_0_ = bf16[64,2048]{1,0:T(8,128)(2,1)S(1)} collective-permute-done((bf16[64,2048]{1,0:T(8,128)(2,1)S(1)}, bf16[64,2048]{1,0:T(8,128)(2,1)S(1)}, u32[]{:S(2)}, u32[]{:S(2)}) %collective-permute-start.30) | collective-permute-done | bytes 262176 | tf_op jit(solution)/shard_map/ppermute | solution.py:341
  91.9 1.7 %collective-permute-start.33 = (bf16[32,2048]{1,0:T(8,128)(2,1)S(1)}, bf16[32,2048]{1,0:T(8,128)(2,1)S(1)}, u32[]{:S(2)}, u32[]{:S(2)}) collective-permute-start(bf16[32,2048]{1,0:T(8,128)(2,1)S(1)} %get-tuple-element.134), channel_id=1, source_target_pairs={{0,6},{1,7},{2,4},{3,5},{4,2},{5,3},{6,0},{7,1},{8,14},{9,15},{10,... | collective-permute-start | bytes 393224 | tf_op jit(solution)/shard_map/ppermute | solution.py:341
  93.7 2.8 %collective-permute-done.31.refs_1_ = bf16[32,2048]{1,0:T(8,128)(2,1)S(1)} collective-permute-done((bf16[32,2048]{1,0:T(8,128)(2,1)S(1)}, bf16[32,2048]{1,0:T(8,128)(2,1)S(1)}, u32[]{:S(2)}, u32[]{:S(2)}) %collective-permute-start.31) | collective-permute-done | bytes 131104 | tf_op jit(solution)/shard_map/ppermute | solution.py:341
  96.5 2.0 %collective-permute-done.32.refs_2_ = bf16[32,2048]{1,0:T(8,128)(2,1)S(1)} collective-permute-done((bf16[32,2048]{1,0:T(8,128)(2,1)S(1)}, bf16[32,2048]{1,0:T(8,128)(2,1)S(1)}, u32[]{:S(2)}, u32[]{:S(2)}) %collective-permute-start.32) | collective-permute-done | bytes 131104 | tf_op jit(solution)/shard_map/ppermute | solution.py:341
  98.6 3.4 %shard_map.142 = (bf16[128,2048]{1,0:T(8,128)(2,1)S(1)}, bf16[128,2048]{1,0:T(8,128)(2,1)S(1)}) custom-call(bf16[64,2048]{1,0:T(8,128)(2,1)S(1)} %get-tuple-element.104.refs_0_, bf16[64,2048]{1,0:T(8,128)(2,1)S(1)} %collective-permute-done.11.refs_1_, bf16[64,2048]{1,0:T(8,128)(2,1)S(1)} %collective-permute-done.12.refs_2_, ...), custom_call_target="tpu_custom_call" | custom-call | flops 76800000 | bytes 15360000 | tf_op jit(solution)/shard_map/pallas_call | solution.py:398
  102.6 1.9 %shard_map.147 = (bf16[64,2048]{1,0:T(8,128)(2,1)S(1)}, bf16[64,2048]{1,0:T(8,128)(2,1)S(1)}) custom-call(bf16[32,2048]{1,0:T(8,128)(2,1)S(1)} %get-tuple-element.119.refs_0_, bf16[32,2048]{1,0:T(8,128)(2,1)S(1)} %collective-permute-done.21.refs_1_, bf16[32,2048]{1,0:T(8,128)(2,1)S(1)} %collective-permute-done.22.refs_2_, ...), custom_call_target="tpu_custom_call" | custom-call | flops 38400000 | bytes 7680000 | tf_op jit(solution)/shard_map/pallas_call | solution.py:398
  104.5 1.9 %shard_map.152 = (bf16[64,2048]{1,0:T(8,128)(2,1)S(1)}, bf16[64,2048]{1,0:T(8,128)(2,1)S(1)}) custom-call(bf16[32,2048]{1,0:T(8,128)(2,1)S(1)} %get-tuple-element.131.refs_0_, bf16[32,2048]{1,0:T(8,128)(2,1)S(1)} %collective-permute-done.31.refs_1_, bf16[32,2048]{1,0:T(8,128)(2,1)S(1)} %collective-permute-done.32.refs_2_, ...), custom_call_target="tpu_custom_call" | custom-call | flops 38400000 | bytes 7680000 | tf_op jit(solution)/shard_map/pallas_call | solution.py:398
  107.0 1.4 collective-permute-start.26
  110.6 1.4 collective-permute-start.36
  114.3 2.5 %collective-permute-done.27.refs_3_ = bf16[32,2048]{1,0:T(8,128)(2,1)S(1)} collective-permute-done((bf16[32,2048]{1,0:T(8,128)(2,1)S(1)}, bf16[32,2048]{1,0:T(8,128)(2,1)S(1)}, u32[]{:S(2)}, u32[]{:S(2)}) %collective-permute-start.27) | collective-permute-done | bytes 131104 | tf_op jit(solution)/shard_map/ppermute | solution.py:341
  119.1 1.7 %collective-permute-start.38 = (bf16[32,2048]{1,0:T(8,128)(2,1)S(1)}, bf16[32,2048]{1,0:T(8,128)(2,1)S(1)}, u32[]{:S(2)}, u32[]{:S(2)}) collective-permute-start(bf16[32,2048]{1,0:T(8,128)(2,1)S(1)} %get-tuple-element.140), channel_id=1, source_target_pairs={{0,6},{1,7},{2,4},{3,5},{4,2},{5,3},{6,0},{7,1},{8,14},{9,15},{10,... | collective-permute-start | bytes 393224 | tf_op jit(solution)/shard_map/ppermute | solution.py:341
  121.1 12.1 %collective-permute-done.37.refs_3_ = bf16[32,2048]{1,0:T(8,128)(2,1)S(1)} collective-permute-done((bf16[32,2048]{1,0:T(8,128)(2,1)S(1)}, bf16[32,2048]{1,0:T(8,128)(2,1)S(1)}, u32[]{:S(2)}, u32[]{:S(2)}) %collective-permute-start.37) | collective-permute-done | bytes 131104 | tf_op jit(solution)/shard_map/ppermute | solution.py:341
  133.2 5.4 %collective-permute-start.29 = (bf16[64,2048]{1,0:T(8,128)(2,1)S(1)}, bf16[64,2048]{1,0:T(8,128)(2,1)S(1)}, u32[]{:S(2)}, u32[]{:S(2)}) collective-permute-start(bf16[64,2048]{1,0:T(8,128)(2,1)S(1)} %shard_map.149), channel_id=1, source_target_pairs={{0,16},{1,17},{2,18},{3,19},{4,20},{5,21},{6,22},{7,23},{8,24},{9,... | collective-permute-start | bytes 786440 | tf_op jit(solution)/shard_map/ppermute | solution.py:341
  141.3 9.8 %collective-permute-done.29.refs_2_ = bf16[64,2048]{1,0:T(8,128)(2,1)S(1)} collective-permute-done((bf16[64,2048]{1,0:T(8,128)(2,1)S(1)}, bf16[64,2048]{1,0:T(8,128)(2,1)S(1)}, u32[]{:S(2)}, u32[]{:S(2)}) %collective-permute-start.29) | collective-permute-done | bytes 262176 | tf_op jit(solution)/shard_map/ppermute | solution.py:341
  151.8 1.5 %shard_map.155 = bf16[1,128,2048]{2,1,0:T(8,128)(2,1)} custom-call(bf16[64,2048]{1,0:T(8,128)(2,1)S(1)} %get-tuple-element.115.refs_0_, bf16[64,2048]{1,0:T(8,128)(2,1)S(1)} %collective-permute-done.19.refs_1_, bf16[64,2048]{1,0:T(8,128)(2,1)S(1)} %collective-permute-done.29.refs_2_, bf16[64,2048]{1,0:T(8,128)(2,1)S(1)} %collective-permute-done.39.refs_3_, ...), custom_call_target="tpu_custom_call" | custom-call | flops 15000000 | bytes 3000000 | tf_op jit(solution)/shard_map/pallas_call | solution.py:441
  (85 shorter events, 31.1 us)
Async XLA Ops:
  4.6 16.0 %collective-permute-start = (bf16[400,128]{1,0:T(8,128)(2,1)S(1)}, bf16[400,128]{1,0:T(8,128)(2,1)S(1)}, u32[]{:S(2)}, u32[]{:S(2)}) collective-permute-start(bf16[400,128]{1,0:T(8,128)(2,1)S(1)} %get-tuple-element.75), channel_id=1, source_target_pairs={{0,4},{1,5},{2,6},{3,7},{4,0},{5,1},{6,2},{7,3},{8,12},{9,13},{10,... | collective-permute-start | bytes 307208 | tf_op jit(solution)/shard_map/ppermute | solution.py:341
  7.6 15.9 %collective-permute-start.1 = (bf16[400,128]{1,0:T(8,128)(2,1)S(1)}, bf16[400,128]{1,0:T(8,128)(2,1)S(1)}, u32[]{:S(2)}, u32[]{:S(2)}) collective-permute-start(bf16[400,128]{1,0:T(8,128)(2,1)S(1)} %get-tuple-element.76), channel_id=1, source_target_pairs={{0,8},{1,9},{2,10},{3,11},{4,12},{5,13},{6,14},{7,15},{8,0},{9,1},... | collective-permute-start | bytes 307208 | tf_op jit(solution)/shard_map/ppermute | solution.py:341
  16.4 8.2 %collective-permute-start.2 = (bf16[400,128]{1,0:T(8,128)(2,1)S(1)}, bf16[400,128]{1,0:T(8,128)(2,1)S(1)}, u32[]{:S(2)}, u32[]{:S(2)}) collective-permute-start(bf16[400,128]{1,0:T(8,128)(2,1)S(1)} %get-tuple-element.77), channel_id=1, source_target_pairs={{0,12},{1,13},{2,14},{3,15},{4,8},{5,9},{6,10},{7,11},{8,4},{9,5},... | collective-permute-start | bytes 307208 | tf_op jit(solution)/shard_map/ppermute | solution.py:341
  17.0 13.0 %collective-permute-start.3 = (bf16[400,128]{1,0:T(8,128)(2,1)S(1)}, bf16[400,128]{1,0:T(8,128)(2,1)S(1)}, u32[]{:S(2)}, u32[]{:S(2)}) collective-permute-start(bf16[400,128]{1,0:T(8,128)(2,1)S(1)} %get-tuple-element.78), channel_id=1, source_target_pairs={{0,16},{1,17},{2,18},{3,19},{4,20},{5,21},{6,22},{7,23},{8,24},{9,... | collective-permute-start | bytes 307208 | tf_op jit(solution)/shard_map/ppermute | solution.py:341
  20.6 13.0 %collective-permute-start.4 = (bf16[400,128]{1,0:T(8,128)(2,1)S(1)}, bf16[400,128]{1,0:T(8,128)(2,1)S(1)}, u32[]{:S(2)}, u32[]{:S(2)}) collective-permute-start(bf16[400,128]{1,0:T(8,128)(2,1)S(1)} %get-tuple-element.79), channel_id=1, source_target_pairs={{0,20},{1,21},{2,22},{3,23},{4,16},{5,17},{6,18},{7,19},{8,28},{9,... | collective-permute-start | bytes 307208 | tf_op jit(solution)/shard_map/ppermute | solution.py:341
  20.6 13.0 %collective-permute-start.5 = (bf16[400,128]{1,0:T(8,128)(2,1)S(1)}, bf16[400,128]{1,0:T(8,128)(2,1)S(1)}, u32[]{:S(2)}, u32[]{:S(2)}) collective-permute-start(bf16[400,128]{1,0:T(8,128)(2,1)S(1)} %get-tuple-element.80), channel_id=1, source_target_pairs={{0,24},{1,25},{2,26},{3,27},{4,28},{5,29},{6,30},{7,31},{8,16},{9,... | collective-permute-start | bytes 307208 | tf_op jit(solution)/shard_map/ppermute | solution.py:341
  23.5 10.0 %collective-permute-start.6 = (bf16[400,128]{1,0:T(8,128)(2,1)S(1)}, bf16[400,128]{1,0:T(8,128)(2,1)S(1)}, u32[]{:S(2)}, u32[]{:S(2)}) collective-permute-start(bf16[400,128]{1,0:T(8,128)(2,1)S(1)} %get-tuple-element.81), channel_id=1, source_target_pairs={{0,28},{1,29},{2,30},{3,31},{4,24},{5,25},{6,26},{7,27},{8,20},{9,... | collective-permute-start | bytes 307208 | tf_op jit(solution)/shard_map/ppermute | solution.py:341
  60.8 6.4 %collective-permute-start.10 = (bf16[64,2048]{1,0:T(8,128)(2,1)S(1)}, bf16[64,2048]{1,0:T(8,128)(2,1)S(1)}, u32[]{:S(2)}, u32[]{:S(2)}) collective-permute-start(bf16[64,2048]{1,0:T(8,128)(2,1)S(1)} %get-tuple-element.103), channel_id=1, source_target_pairs={{0,8},{1,9},{2,10},{3,11},{4,12},{5,13},{6,14},{7,15},{8,0},{9,1},... | collective-permute-start | bytes 786440 | tf_op jit(solution)/shard_map/ppermute | solution.py:341
  67.9 7.1 %collective-permute-start.11 = (bf16[64,2048]{1,0:T(8,128)(2,1)S(1)}, bf16[64,2048]{1,0:T(8,128)(2,1)S(1)}, u32[]{:S(2)}, u32[]{:S(2)}) collective-permute-start(bf16[64,2048]{1,0:T(8,128)(2,1)S(1)} %get-tuple-element.105), channel_id=1, source_target_pairs={{0,2},{1,3},{2,0},{3,1},{4,6},{5,7},{6,4},{7,5},{8,10},{9,11},{10,... | collective-permute-start | bytes 786440 | tf_op jit(solution)/shard_map/ppermute | solution.py:341
  69.5 9.6 %collective-permute-start.12 = (bf16[64,2048]{1,0:T(8,128)(2,1)S(1)}, bf16[64,2048]{1,0:T(8,128)(2,1)S(1)}, u32[]{:S(2)}, u32[]{:S(2)}) collective-permute-start(bf16[64,2048]{1,0:T(8,128)(2,1)S(1)} %get-tuple-element.106), channel_id=1, source_target_pairs={{0,4},{1,5},{2,6},{3,7},{4,0},{5,1},{6,2},{7,3},{8,12},{9,13},{10,... | collective-permute-start | bytes 786440 | tf_op jit(solution)/shard_map/ppermute | solution.py:341
  70.6 8.5 %collective-permute-start.13 = (bf16[64,2048]{1,0:T(8,128)(2,1)S(1)}, bf16[64,2048]{1,0:T(8,128)(2,1)S(1)}, u32[]{:S(2)}, u32[]{:S(2)}) collective-permute-start(bf16[64,2048]{1,0:T(8,128)(2,1)S(1)} %get-tuple-element.107), channel_id=1, source_target_pairs={{0,6},{1,7},{2,4},{3,5},{4,2},{5,3},{6,0},{7,1},{8,14},{9,15},{10,... | collective-permute-start | bytes 786440 | tf_op jit(solution)/shard_map/ppermute | solution.py:341
  71.5 9.6 %collective-permute-start.20 = (bf16[64,2048]{1,0:T(8,128)(2,1)S(1)}, bf16[64,2048]{1,0:T(8,128)(2,1)S(1)}, u32[]{:S(2)}, u32[]{:S(2)}) collective-permute-start(bf16[64,2048]{1,0:T(8,128)(2,1)S(1)} %get-tuple-element.118), channel_id=1, source_target_pairs={{0,16},{1,17},{2,18},{3,19},{4,20},{5,21},{6,22},{7,23},{8,24},{9,... | collective-permute-start | bytes 786440 | tf_op jit(solution)/shard_map/ppermute | solution.py:341
  79.1 19.5 %collective-permute-start.14 = (bf16[128,2048]{1,0:T(8,128)(2,1)S(1)}, bf16[128,2048]{1,0:T(8,128)(2,1)S(1)}, u32[]{:S(2)}, u32[]{:S(2)}) collective-permute-start(bf16[128,2048]{1,0:T(8,128)(2,1)S(1)} %shard_map.141), channel_id=1, source_target_pairs={{0,1},{1,0},{2,3},{3,2},{4,5},{5,4},{6,7},{7,6},{8,9},{9,8},{10,11... | collective-permute-start | bytes 1572872 | tf_op jit(solution)/shard_map/ppermute | solution.py:341
  79.2 10.6 %collective-permute-start.30 = (bf16[64,2048]{1,0:T(8,128)(2,1)S(1)}, bf16[64,2048]{1,0:T(8,128)(2,1)S(1)}, u32[]{:S(2)}, u32[]{:S(2)}) collective-permute-start(bf16[64,2048]{1,0:T(8,128)(2,1)S(1)} %get-tuple-element.130), channel_id=1, source_target_pairs={{0,24},{1,25},{2,26},{3,27},{4,28},{5,29},{6,30},{7,31},{8,16},{9,... | collective-permute-start | bytes 786440 | tf_op jit(solution)/shard_map/ppermute | solution.py:341
  81.4 9.3 %collective-permute-start.21 = (bf16[32,2048]{1,0:T(8,128)(2,1)S(1)}, bf16[32,2048]{1,0:T(8,128)(2,1)S(1)}, u32[]{:S(2)}, u32[]{:S(2)}) collective-permute-start(bf16[32,2048]{1,0:T(8,128)(2,1)S(1)} %get-tuple-element.120), channel_id=1, source_target_pairs={{0,2},{1,3},{2,0},{3,1},{4,6},{5,7},{6,4},{7,5},{8,10},{9,11},{10,... | collective-permute-start | bytes 393224 | tf_op jit(solution)/shard_map/ppermute | solution.py:341
  83.0 9.0 %collective-permute-start.22 = (bf16[32,2048]{1,0:T(8,128)(2,1)S(1)}, bf16[32,2048]{1,0:T(8,128)(2,1)S(1)}, u32[]{:S(2)}, u32[]{:S(2)}) collective-permute-start(bf16[32,2048]{1,0:T(8,128)(2,1)S(1)} %get-tuple-element.121), channel_id=1, source_target_pairs={{0,4},{1,5},{2,6},{3,7},{4,0},{5,1},{6,2},{7,3},{8,12},{9,13},{10,... | collective-permute-start | bytes 393224 | tf_op jit(solution)/shard_map/ppermute | solution.py:341
  84.3 9.3 %collective-permute-start.23 = (bf16[32,2048]{1,0:T(8,128)(2,1)S(1)}, bf16[32,2048]{1,0:T(8,128)(2,1)S(1)}, u32[]{:S(2)}, u32[]{:S(2)}) collective-permute-start(bf16[32,2048]{1,0:T(8,128)(2,1)S(1)} %get-tuple-element.122), channel_id=1, source_target_pairs={{0,6},{1,7},{2,4},{3,5},{4,2},{5,3},{6,0},{7,1},{8,14},{9,15},{10,... | collective-permute-start | bytes 393224 | tf_op jit(solution)/shard_map/ppermute | solution.py:341
  90.7 7.8 %collective-permute-start.32 = (bf16[32,2048]{1,0:T(8,128)(2,1)S(1)}, bf16[32,2048]{1,0:T(8,128)(2,1)S(1)}, u32[]{:S(2)}, u32[]{:S(2)}) collective-permute-start(bf16[32,2048]{1,0:T(8,128)(2,1)S(1)} %get-tuple-element.133), channel_id=1, source_target_pairs={{0,4},{1,5},{2,6},{3,7},{4,0},{5,1},{6,2},{7,3},{8,12},{9,13},{10,... | collective-permute-start | bytes 393224 | tf_op jit(solution)/shard_map/ppermute | solution.py:341
  91.9 6.5 %collective-permute-start.33 = (bf16[32,2048]{1,0:T(8,128)(2,1)S(1)}, bf16[32,2048]{1,0:T(8,128)(2,1)S(1)}, u32[]{:S(2)}, u32[]{:S(2)}) collective-permute-start(bf16[32,2048]{1,0:T(8,128)(2,1)S(1)} %get-tuple-element.134), channel_id=1, source_target_pairs={{0,6},{1,7},{2,4},{3,5},{4,2},{5,3},{6,0},{7,1},{8,14},{9,15},{10,... | collective-permute-start | bytes 393224 | tf_op jit(solution)/shard_map/ppermute | solution.py:341
  93.7 8.9 %collective-permute-start.24 = (bf16[64,2048]{1,0:T(8,128)(2,1)S(1)}, bf16[64,2048]{1,0:T(8,128)(2,1)S(1)}, u32[]{:S(2)}, u32[]{:S(2)}) collective-permute-start(bf16[64,2048]{1,0:T(8,128)(2,1)S(1)} %shard_map.146), channel_id=1, source_target_pairs={{0,1},{1,0},{2,3},{3,2},{4,5},{5,4},{6,7},{7,6},{8,9},{9,8},{10,11... | collective-permute-start | bytes 786440 | tf_op jit(solution)/shard_map/ppermute | solution.py:341
  102.0 10.0 %collective-permute-start.15 = (bf16[128,2048]{1,0:T(8,128)(2,1)S(1)}, bf16[128,2048]{1,0:T(8,128)(2,1)S(1)}, u32[]{:S(2)}, u32[]{:S(2)}) collective-permute-start(bf16[128,2048]{1,0:T(8,128)(2,1)S(1)} %get-tuple-element.110), channel_id=1, source_target_pairs={{0,1},{1,0},{2,3},{3,2},{4,5},{5,4},{6,7},{7,6},{8,9},{9,8},{10,11... | collective-permute-start | bytes 1572872 | tf_op jit(solution)/shard_map/ppermute | solution.py:341
  108.4 8.4 %collective-permute-start.27 = (bf16[32,2048]{1,0:T(8,128)(2,1)S(1)}, bf16[32,2048]{1,0:T(8,128)(2,1)S(1)}, u32[]{:S(2)}, u32[]{:S(2)}) collective-permute-start(bf16[32,2048]{1,0:T(8,128)(2,1)S(1)} %get-tuple-element.127), channel_id=1, source_target_pairs={{0,4},{1,5},{2,6},{3,7},{4,0},{5,1},{6,2},{7,3},{8,12},{9,13},{10,... | collective-permute-start | bytes 393224 | tf_op jit(solution)/shard_map/ppermute | solution.py:341
  109.3 7.4 %collective-permute-start.28 = (bf16[32,2048]{1,0:T(8,128)(2,1)S(1)}, bf16[32,2048]{1,0:T(8,128)(2,1)S(1)}, u32[]{:S(2)}, u32[]{:S(2)}) collective-permute-start(bf16[32,2048]{1,0:T(8,128)(2,1)S(1)} %get-tuple-element.128), channel_id=1, source_target_pairs={{0,6},{1,7},{2,4},{3,5},{4,2},{5,3},{6,0},{7,1},{8,14},{9,15},{10,... | collective-permute-start | bytes 393224 | tf_op jit(solution)/shard_map/ppermute | solution.py:341
  110.6 8.5 %collective-permute-start.36 = (bf16[32,2048]{1,0:T(8,128)(2,1)S(1)}, bf16[32,2048]{1,0:T(8,128)(2,1)S(1)}, u32[]{:S(2)}, u32[]{:S(2)}) collective-permute-start(bf16[32,2048]{1,0:T(8,128)(2,1)S(1)} %get-tuple-element.138), channel_id=1, source_target_pairs={{0,2},{1,3},{2,0},{3,1},{4,6},{5,7},{6,4},{7,5},{8,10},{9,11},{10,... | collective-permute-start | bytes 393224 | tf_op jit(solution)/shard_map/ppermute | solution.py:341
  112.1 28.2 %collective-permute-start.16 = (bf16[64,2048]{1,0:T(8,128)(2,1)S(1)}, bf16[64,2048]{1,0:T(8,128)(2,1)S(1)}, u32[]{:S(2)}, u32[]{:S(2)}) collective-permute-start(bf16[64,2048]{1,0:T(8,128)(2,1)S(1)} %get-tuple-element.112), channel_id=1, source_target_pairs={{0,2},{1,3},{2,0},{3,1},{4,6},{5,7},{6,4},{7,5},{8,10},{9,11},{10,... | collective-permute-start | bytes 786440 | tf_op jit(solution)/shard_map/ppermute | solution.py:341
  113.1 27.2 %collective-permute-start.17 = (bf16[64,2048]{1,0:T(8,128)(2,1)S(1)}, bf16[64,2048]{1,0:T(8,128)(2,1)S(1)}, u32[]{:S(2)}, u32[]{:S(2)}) collective-permute-start(bf16[64,2048]{1,0:T(8,128)(2,1)S(1)} %get-tuple-element.113), channel_id=1, source_target_pairs={{0,4},{1,5},{2,6},{3,7},{4,0},{5,1},{6,2},{7,3},{8,12},{9,13},{10,... | collective-permute-start | bytes 786440 | tf_op jit(solution)/shard_map/ppermute | solution.py:341
  116.8 23.5 %collective-permute-start.18 = (bf16[64,2048]{1,0:T(8,128)(2,1)S(1)}, bf16[64,2048]{1,0:T(8,128)(2,1)S(1)}, u32[]{:S(2)}, u32[]{:S(2)}) collective-permute-start(bf16[64,2048]{1,0:T(8,128)(2,1)S(1)} %get-tuple-element.114), channel_id=1, source_target_pairs={{0,6},{1,7},{2,4},{3,5},{4,2},{5,3},{6,0},{7,1},{8,14},{9,15},{10,... | collective-permute-start | bytes 786440 | tf_op jit(solution)/shard_map/ppermute | solution.py:341
  116.8 16.4 %collective-permute-start.37 = (bf16[32,2048]{1,0:T(8,128)(2,1)S(1)}, bf16[32,2048]{1,0:T(8,128)(2,1)S(1)}, u32[]{:S(2)}, u32[]{:S(2)}) collective-permute-start(bf16[32,2048]{1,0:T(8,128)(2,1)S(1)} %get-tuple-element.139), channel_id=1, source_target_pairs={{0,4},{1,5},{2,6},{3,7},{4,0},{5,1},{6,2},{7,3},{8,12},{9,13},{10,... | collective-permute-start | bytes 393224 | tf_op jit(solution)/shard_map/ppermute | solution.py:341
  119.1 19.5 %collective-permute-start.38 = (bf16[32,2048]{1,0:T(8,128)(2,1)S(1)}, bf16[32,2048]{1,0:T(8,128)(2,1)S(1)}, u32[]{:S(2)}, u32[]{:S(2)}) collective-permute-start(bf16[32,2048]{1,0:T(8,128)(2,1)S(1)} %get-tuple-element.140), channel_id=1, source_target_pairs={{0,6},{1,7},{2,4},{3,5},{4,2},{5,3},{6,0},{7,1},{8,14},{9,15},{10,... | collective-permute-start | bytes 393224 | tf_op jit(solution)/shard_map/ppermute | solution.py:341
  133.2 17.9 %collective-permute-start.29 = (bf16[64,2048]{1,0:T(8,128)(2,1)S(1)}, bf16[64,2048]{1,0:T(8,128)(2,1)S(1)}, u32[]{:S(2)}, u32[]{:S(2)}) collective-permute-start(bf16[64,2048]{1,0:T(8,128)(2,1)S(1)} %shard_map.149), channel_id=1, source_target_pairs={{0,16},{1,17},{2,18},{3,19},{4,20},{5,21},{6,22},{7,23},{8,24},{9,... | collective-permute-start | bytes 786440 | tf_op jit(solution)/shard_map/ppermute | solution.py:341
  139.0 12.1 %collective-permute-start.39 = (bf16[64,2048]{1,0:T(8,128)(2,1)S(1)}, bf16[64,2048]{1,0:T(8,128)(2,1)S(1)}, u32[]{:S(2)}, u32[]{:S(2)}) collective-permute-start(bf16[64,2048]{1,0:T(8,128)(2,1)S(1)} %shard_map.154), channel_id=1, source_target_pairs={{0,24},{1,25},{2,26},{3,27},{4,28},{5,29},{6,30},{7,31},{8,16},{9,... | collective-permute-start | bytes 786440 | tf_op jit(solution)/shard_map/ppermute | solution.py:341
  141.2 10.6 %collective-permute-start.19 = (bf16[64,2048]{1,0:T(8,128)(2,1)S(1)}, bf16[64,2048]{1,0:T(8,128)(2,1)S(1)}, u32[]{:S(2)}, u32[]{:S(2)}) collective-permute-start(bf16[64,2048]{1,0:T(8,128)(2,1)S(1)} %get-tuple-element.116), channel_id=1, source_target_pairs={{0,8},{1,9},{2,10},{3,11},{4,12},{5,13},{6,14},{7,15},{8,0},{9,1},... | collective-permute-start | bytes 786440 | tf_op jit(solution)/shard_map/ppermute | solution.py:341
  (14 other events, 121.5 us)

commit v2 on v1

v2 whole, which is shorter than its diff:
```python
import functools
import math

import jax
import jax.numpy as jnp
from jax import lax
from jax.experimental import pallas as pl
from jax.experimental.pallas import tpu as pltpu
from jax.sharding import PartitionSpec as P


HD = 64
GROUPS = 4
CORES = 2
CHUNKS = ((2,), (3,), (1,), (0,))
norm_eps = 1e-05
F32 = jnp.float32
BF16 = jnp.bfloat16
MB = 1024 * 1024
FLOPS = 1.5e7
BYTES = 3.0e6

VM = pl.BlockSpec(memory_space=pltpu.VMEM)
SM = pl.BlockSpec(memory_space=pltpu.SMEM)
HB = pl.BlockSpec(memory_space=pltpu.HBM)
NT = (((1,), (1,)), ((), ()))


def call(body, out, n_in, scratch=(), limit=8, in_specs=None, us=1.0):
    return pl.pallas_call(
        body,
        out_shape=out,
        in_specs=in_specs or [VM] * n_in,
        out_specs=jax.tree.map(lambda _: VM, out),
        scratch_shapes=list(scratch),
        compiler_params=pltpu.CompilerParams(vmem_limit_bytes=limit * MB),
        cost_estimate=pl.CostEstimate(flops=int(us * FLOPS), bytes_accessed=int(us * BYTES), transcendentals=0),
    )


def in_hbm(array):
    return pltpu.with_memory_space_constraint(array, pltpu.HBM)


def iota(shape, dim):
    return lax.broadcasted_iota(jnp.int32, shape, dim)


def pack_body(q_ref, k_ref, v_ref, ks_ref, out_ref):
    n, rows, cols = out_ref.shape
    tokens, heads = ks_ref.shape[1], ks_ref.shape[2]
    local = heads // n
    pieces = tokens // cols
    eye = (iota((heads, heads), 0) == iota((heads, heads), 1)).astype(BF16)
    shift = lax.dot_general(eye, ks_ref[0], NT, preferred_element_type=F32)
    pad = rows - 3 * tokens
    for d in range(n):
        lanes = slice(d * cols, (d + 1) * cols)
        out_ref[d, 0:tokens, :] = q_ref[0, :, lanes]
        out_ref[d, tokens : 2 * tokens, :] = k_ref[0, :, lanes]
        out_ref[d, 2 * tokens : 3 * tokens, :] = v_ref[0, :, lanes]
        tail = [
            shift[d * local + h : d * local + h + 1, p * cols : (p + 1) * cols]
            for h in range(local)
            for p in range(pieces)
        ]
        tail.append(jnp.zeros((pad - len(tail), cols), F32))
        out_ref[d, 3 * tokens :, :] = jnp.concatenate(tail, axis=0).astype(BF16)


def pick_body(me_ref, q_ref, k_ref, v_ref, ks_ref, route_ref, rw_ref, *refs, plane, cap):
    out_refs, (line_ref, table_ref, meta_ref) = refs[:-8], refs[-8:-5]
    ks_in, route_in, rw_in, sems, small_sems = refs[-5:]
    small = [
        pltpu.make_async_copy(source, target, small_sems.at[i])
        for i, (source, target) in enumerate(
            ((ks_ref, ks_in), (route_ref, route_in), (rw_ref, rw_in))
        )
    ]
    for copy in small:
        copy.start()
    _, cols = out_refs[0].shape
    heads, tokens = ks_in.shape[1], ks_in.shape[2]
    local = heads // len(out_refs)
    step = len(out_refs) // GROUPS
    copies = []
    for k, out_ref in enumerate(out_refs):
        lanes = pl.ds(pl.multiple_of((me_ref[1] ^ k) * cols, cols), cols)
        for part, ref in enumerate((q_ref, k_ref, v_ref)):
            copies.append(
                pltpu.make_async_copy(
                    ref.at[0, :, lanes],
                    out_ref.at[part * tokens : (part + 1) * tokens, :],
                    sems.at[k, part],
                )
            )
    for copy in copies:
        copy.start()
    for copy in small:
        copy.wait()
    line_ref[...], table_ref[...], metas = routing(me_ref, route_in[0], rw_in[0], plane, cap)
    meta_ref[...] = metas[0]
    line, head = iota((8, heads), 0), iota((8, heads), 1)
    for k, out_ref in enumerate(out_refs):
        take = (head == line + (me_ref[1] ^ k) * local) & (line < local)
        shift = jnp.dot(take.astype(F32).astype(BF16), ks_in[0], preferred_element_type=F32)
        out_ref[3 * tokens : 3 * tokens + 8, :] = shift.astype(BF16)
        out_ref[3 * tokens + 8 :, :] = (
            metas[k // step] if k % step == 0 else jnp.zeros((8, cols), BF16)
        )
    for copy in copies:
        copy.wait()


def fetch_body(*refs):
    half = len(refs) // 2
    copies = [
        pltpu.make_async_copy(source, target, refs[-1].at[i])
        for i, (source, target) in enumerate(zip(refs[:half], refs[half : 2 * half]))
    ]
    for copy in copies:
        copy.start()
    for copy in copies:
        copy.wait()


def attend(me_ref, hs_ref, x_ref, scratch, row_at, key_at, count, diagonal, carries):
    z_ref, b_ref, w_ref = scratch
    cols = x_ref.shape[2]
    tokens = z_ref.shape[1]
    local, pieces = cols // HD, tokens // cols
    span = count * tokens
    lane = iota((tokens, cols), 1) // HD
    keys = x_ref[pl.ds(key_at, count), tokens : 2 * tokens, :].reshape(span, cols)
    values = x_ref[pl.ds(key_at, count), 2 * tokens : 3 * tokens, :].reshape(span, cols)
    row, col = iota((2 * tokens, 2 * tokens), 0), iota((2 * tokens, 2 * tokens), 1)
    summing = jnp.where((col >= tokens) | (row % tokens >= col), 1.0, 0.0).astype(BF16)
    causal = iota((tokens, tokens), 1) < iota((tokens, tokens), 0)
    for h in range(local):
        q = x_ref[row_at, 0:tokens, :].astype(F32) * (1.0 / math.sqrt(HD))
        q = jnp.where(lane == h, q, 0.0).astype(BF16)
        logits = lax.dot_general(q, keys, NT, preferred_element_type=F32)
        base = 3 * tokens + h * pieces
        for j in range(count):
            at = slice(j * tokens, (j + 1) * tokens)
            off = [x_ref[key_at + j, base + p : base + p + 1, :] for p in range(pieces)]
            off = off[0] if pieces == 1 else jnp.concatenate(off, axis=1)
            z = logits[:, at] + (off.astype(F32) + hs_ref[me_ref[1] * local + h])
            z_ref[h, :, at] = z
            breaks = -(jnp.maximum(z, 0.0) + jnp.log(1.0 + jnp.exp(-jnp.abs(z))))
            if diagonal and j == count - 1:
                breaks = jnp.where(causal, breaks, 0.0)
            high = breaks.astype(BF16)
            tile = slice((h * count + j) * tokens, (h * count + j + 1) * tokens)
            b_ref[tile, 0:tokens] = high
            b_ref[tile, tokens:] = (breaks - high.astype(F32)).astype(BF16)
    sums = jnp.dot(b_ref[0 : local * span, :], summing, preferred_element_type=F32)
    total, totals = None, []
    for h in range(local):
        carry = carries[h] if carries else None
        for j in range(count - 1, -1, -1):
            at = slice(j * tokens, (j + 1) * tokens)
            tile = slice((h * count + j) * tokens, (h * count + j + 1) * tokens)
            power = z_ref[h, :, at] + sums[tile, 0:tokens]
            if carry is not None:
                power = power + carry
            weight = jnp.exp(power)
            if diagonal and j == count - 1:
                weight = jnp.where(causal, weight, 0.0)
            w_ref[h, :, at] = weight.astype(BF16)
            part = sums[tile, tokens:]
            carry = part if carry is None else carry + part
        totals.append(carry)
        got = jnp.dot(w_ref[h, :, 0:span], values, preferred_element_type=F32)
        total = got if total is None else jnp.where(lane == h, got, total)
    return total, totals


def near_body(me_ref, hs_ref, *refs):
    x_refs, (part_ref, carry_ref, x_ref), scratch = refs[:-6], refs[-6:-3], refs[-3:]
    half = len(x_refs)
    for k, ref in enumerate(x_refs):
        x_ref[(me_ref[1] & (half - 1)) ^ k] = ref[...]
    for i in range(half):
        total, totals = attend(me_ref, hs_ref, x_ref, scratch, i, 0, i + 1, True, None)
        part_ref[i] = total
        for h, carry in enumerate(totals):
            carry_ref[i, h] = carry


def attention_body(me_ref, hs_ref, near_ref, near_carry_ref, *refs):
    x_refs, (out_ref, x_ref, part_ref, carry_ref), scratch = refs[:-7], refs[-7:-3], refs[-3:]
    n = len(x_refs)
    half = n // 2
    for k, ref in enumerate(x_refs):
        x_ref[me_ref[1] ^ k] = ref[...]
    mine = me_ref[1] & half
    other = mine ^ half
    for i in range(half):
        part_ref[mine + i] = near_ref[i]
        carry_ref[mine + i] = near_carry_ref[i]
    for i in range(half):
        total, totals = attend(
            me_ref, hs_ref, x_ref, scratch, other + i, other, i + 1, True, None
        )
        part_ref[other + i] = total
        for h, carry in enumerate(totals):
            carry_ref[other + i, h] = carry
    for i in range(half):
        out_ref[i] = part_ref[i].astype(BF16)
    for i in range(half, n):
        carries = [carry_ref[i, h] for h in range(carry_ref.shape[1])]
        total, _ = attend(me_ref, hs_ref, x_ref, scratch, i, 0, half, False, carries)
        out_ref[i] = (part_ref[i] + total).astype(BF16)


def routing(me_ref, route, weights, plane, cap):
    tokens = route.shape[1]
    bits = plane.bit_length() - 1
    zme, pme = me_ref[0] >> bits, me_ref[0] & (plane - 1)
    eye = iota((tokens, tokens), 0) == iota((tokens, tokens), 1)
    before = (iota((tokens, tokens), 0) < iota((tokens, tokens), 1)).astype(BF16)

    def to_col(line):
        return jnp.sum(jnp.where(eye, line, 0.0), axis=1, keepdims=True)

    def count(hot):
        return jnp.dot(hot.astype(BF16), before, preferred_element_type=F32)

    chosen = [route[k : k + 1].astype(F32) for k in range(2)]
    names = iota((GROUPS * plane, tokens), 0).astype(F32)
    hot = [(names == e).astype(F32) for e in chosen]
    earlier = count(hot[0] + hot[1])
    ranks = [jnp.sum(h * earlier, axis=0, keepdims=True) for h in hot]
    group = route[0:1] >> bits
    in_group = (iota((8, tokens), 0) == group).astype(F32)
    place = jnp.sum(in_group * count(in_group), axis=0, keepdims=True)
    lines = [jnp.where(group == (zme ^ d), place, -1.0) for d in range(GROUPS)]
    cols = [to_col(line) for line in lines]
    lane = iota((tokens, 128), 1)
    table = jnp.zeros((tokens, 128), F32)
    for k, c in enumerate(cols):
        table = jnp.where(lane == k, c, table)
    relay = [
        to_col((((route[k : k + 1] & (plane - 1)) ^ pme) * cap).astype(F32) + ranks[k])
        for k in range(2)
    ]
    shares = [to_col(weights[k : k + 1]) for k in range(2)]
    slot = iota((tokens, tokens), 1).astype(F32)
    metas = []
    for c in cols:
        pick = slot == c

        def gathered(column):
            return jnp.sum(jnp.where(pick, column, 0.0), axis=0, keepdims=True)

        out = [gathered(v + 1.0) - 1.0 for v in relay]
        for share in shares:
            rest = gathered(share)
            for _ in range(3):
                term = rest.astype(BF16).astype(F32)
                out.append(term)
                rest = rest - term
        metas.append(jnp.concatenate(out, axis=0).astype(BF16))
    lines = jnp.concatenate(lines + [jnp.zeros((4, tokens), F32)], axis=0)
    return lines.astype(jnp.int32), table.astype(jnp.int32), metas


def route_body(me_ref, route_ref, rw_ref, line_ref, table_ref, *meta_refs, plane, cap):
    line_ref[...], table_ref[...], metas = routing(
        me_ref, route_ref[0], rw_ref[0], plane, cap
    )
    for ref, meta in zip(meta_refs, metas):
        ref[...] = meta


def hidden_body(att_ref, stream_ref, mg_ref, w_ref, pg_ref, dest_ref, hid_ref, *far_refs):
    n, tokens, cols = att_ref.shape
    pieces = [att_ref[s].astype(F32) for s in range(n)]
    if cols % 128 == 0:
        pieces = [jnp.concatenate(pieces, axis=1)]
    size = pieces[0].shape[1]
    square = sum(jnp.sum(p * p, axis=1, keepdims=True) for p in pieces)
    scale = lax.rsqrt(square / (n * cols) + norm_eps)
    mixed = None
    for s, p in enumerate(pieces):
        at = slice(s * size, (s + 1) * size)
        normed = (p * scale * mg_ref[:, at]).astype(BF16)
        part = jnp.dot(normed, w_ref[at, :], preferred_element_type=F32)
        mixed = part if mixed is None else mixed + part
    summed = stream_ref[0].astype(F32) + mixed
    mean = jnp.mean(summed * summed, axis=1, keepdims=True)
    hidden = (summed * lax.rsqrt(mean + norm_eps) * pg_ref[...]).astype(BF16)
    hid_ref[...] = hidden
    for d, ref in enumerate(far_refs):
        pick = iota((ref.shape[0], tokens), 0) == dest_ref[d : d + 1, :]
        ref[...] = jnp.dot(
            pick.astype(F32).astype(BF16), hidden, preferred_element_type=F32
        ).astype(BF16)


def meta_of(ref):
    return ref[ref.shape[0] - 8 :].astype(F32)


def relay_body(*refs, sources):
    x_refs, meta_refs, out_refs = refs[:sources], refs[sources : 2 * sources], refs[2 * sources :]
    half = x_refs[0].shape[0]
    block = out_refs[0].shape[0]
    slot = iota((block * len(out_refs), half), 0)
    rows = None
    for x_ref, meta_ref in zip(x_refs, meta_refs):
        place = meta_of(meta_ref)[0:2, 0:half].astype(jnp.int32)
        pick = (slot == place[0:1]) | (slot == place[1:2])
        part = jnp.dot(pick.astype(F32).astype(BF16), x_ref[...], preferred_element_type=F32)
        rows = part if rows is None else rows + part
    rows = rows.astype(BF16)
    for m, ref in enumerate(out_refs):
        ref[...] = rows[m * block : (m + 1) * block]


def expert_body(*refs, takes):
    x_refs, (wg_ref, wu_ref, wd_ref), out_refs = (
        refs[: len(takes)],
        refs[len(takes) : len(takes) + 3],
        refs[len(takes) + 3 :],
    )
    parts = [ref[0:take] for ref, take in zip(x_refs, takes)]
    x = parts[0] if len(parts) == 1 else jnp.concatenate(parts, axis=0)
    gate = jnp.dot(x, wg_ref[0], preferred_element_type=F32)
    upper = jnp.dot(x, wu_ref[0], preferred_element_type=F32)
    inner = (gate / (1.0 + jnp.exp(-gate)) * upper).astype(BF16)
    out = jnp.dot(inner, wd_ref[0], preferred_element_type=F32).astype(BF16)
    at = 0
    for ref in out_refs:
        ref[...] = out[at : at + ref.shape[0]]
        at += ref.shape[0]


def second_halves_body(*refs):
    out_ref = refs[-1]
    part = out_ref.shape[0] // (len(refs) - 1)
    for m, ref in enumerate(refs[:-1]):
        out_ref[m * part : (m + 1) * part] = ref[part:]


def join_body(own_ref, back_ref, *out_refs):
    part = out_refs[0].shape[0] // 2
    for m, ref in enumerate(out_refs):
        at = slice(m * part, (m + 1) * part)
        ref[0:part] = own_ref[at]
        ref[part:] = back_ref[at]


def gather_body(*refs, sources):
    meta_refs, row_refs, out_refs = refs[:sources], refs[sources:-sources], refs[-sources:]
    parts = [ref[...] for ref in row_refs]
    rows = parts[0] if len(parts) == 1 else jnp.concatenate(parts, axis=0)
    for meta_ref, out_ref in zip(meta_refs, out_refs):
        half = out_ref.shape[0]
        eye = iota((half, half), 0) == iota((half, half), 1)
        slot = iota((half, rows.shape[0]), 1).astype(F32)
        meta = meta_of(meta_ref)[:, 0:half]
        total = None
        for k in range(2):
            share = meta[2 + 3 * k : 3 + 3 * k]
            for r in range(3 + 3 * k, 5 + 3 * k):
                share = share + meta[r : r + 1]
            place, weight = [
                jnp.sum(jnp.where(eye, line, 0.0), axis=1, keepdims=True)
                for line in (meta[k : k + 1], share)
            ]
            pick = (slot == place).astype(F32).astype(BF16)
            part = jnp.dot(pick, rows, preferred_element_type=F32) * weight
            total = part if total is None else total + part
        out_ref[...] = total.astype(BF16)


def gathered_body(*refs, first):
    far_refs, (hid_ref, dest_ref, out_ref) = refs[:-3], refs[-3:]
    tokens = hid_ref.shape[0]
    result = hid_ref[...].astype(F32)
    for d, ref in enumerate(far_refs, first):
        slot = iota((tokens, ref.shape[0]), 1)
        hot = (slot == dest_ref[:, d : d + 1]).astype(F32).astype(BF16)
        result = result + jnp.dot(hot, ref[...], preferred_element_type=F32)
    out_ref[...] = result.astype(out_ref.dtype).reshape(out_ref.shape)


def on_device(
    stream,
    queries,
    keys_in,
    values_in,
    key_shift,
    head_shift,
    mix_gain,
    out_weight,
    post_gain,
    route,
    route_weight,
    w_gate,
    w_up,
    w_down,
):
    tokens, width = stream.shape[1], stream.shape[2]
    size_sp, size_dp = lax.axis_size("sp"), lax.axis_size("dp")
    heads = key_shift.shape[2]
    local = heads // size_sp
    cols = queries.shape[2] // size_sp
    rows = 3 * tokens + 16
    n_expert = size_sp * size_dp
    plane = n_expert // GROUPS
    chips = plane // CORES
    cap = tokens // plane
    half = tokens // 2
    both = ("sp", "dp")
    sds = jax.ShapeDtypeStruct
    sp = lax.axis_index("sp")
    me = jnp.stack([sp * size_dp + lax.axis_index("dp"), sp]).astype(jnp.int32)

    def swap(array, bit):
        return lax.ppermute(array, both, [(i, i ^ bit) for i in range(n_expert)])

    routes = (route.swapaxes(1, 2), route_weight.swapaxes(1, 2))
    tables = (sds((8, tokens), jnp.int32), sds((tokens, 128), jnp.int32))
    ranked = dict(plane=plane, cap=cap)
    inside = cols == tokens
    if inside:
        *sent, dest_rows, dest_cols, meta = call(
            functools.partial(pick_body, **ranked),
            (sds((rows, cols), BF16),) * size_sp + tables + (sds((8, tokens), BF16),),
            0,
            in_specs=[SM] + [HB] * 6,
            scratch=[
                pltpu.VMEM((1, heads, tokens), BF16),
                pltpu.VMEM((1, 2, tokens), jnp.int32),
                pltpu.VMEM((1, 2, tokens), F32),
                pltpu.SemaphoreType.DMA((size_sp, 3)),
                pltpu.SemaphoreType.DMA((3,)),
            ],
        )(me, *map(in_hbm, (queries, keys_in, values_in, key_shift.swapaxes(1, 2)) + routes))
    else:
        sent = call(pack_body, sds((size_sp, rows, cols), BF16), 4)(
            queries, keys_in, values_in, key_shift
        )
        sent = [
            lax.dynamic_index_in_dim(sent, sp ^ k, 0, keepdims=False) for k in range(size_sp)
        ]
    got = [sent[0]] + [None] * (size_sp - 1)
    for k in range(size_sp - 1, 0, -1):
        got[k] = swap(sent[k], k * size_dp)
    if inside:
        metas = [meta] + [got[d * size_sp // GROUPS] for d in range(1, GROUPS)]
    else:
        dest_rows, dest_cols, *metas = call(
            functools.partial(route_body, **ranked),
            tables + (sds((8, tokens), BF16),) * GROUPS,
            3,
            in_specs=[SM, VM, VM],
        )(me, *routes)
        for d in range(1, GROUPS):
            metas[d] = swap(metas[d], d * plane)
    later = [in_hbm(x) for x in (out_weight, stream, mix_gain[None], post_gain[None], w_down)]
    out_weight, stream, mix_gain, post_gain, w_down = call(
        fetch_body,
        tuple(sds(x.shape, x.dtype) for x in later),
        0,
        in_specs=[HB] * len(later),
        scratch=[pltpu.SemaphoreType.DMA((len(later),))],
        us=5,
    )(*later)
    halved = size_sp // 2
    scratch = [
        pltpu.VMEM((local, tokens, halved * tokens), F32),
        pltpu.VMEM((local * halved * tokens, 2 * tokens), BF16),
        pltpu.VMEM((local, tokens, halved * tokens), BF16),
    ]
    near = call(
        near_body,
        (sds((halved, tokens, cols), F32), sds((halved, local, tokens, tokens), F32)),
        0,
        in_specs=[SM, SM] + [VM] * halved,
        scratch=[pltpu.VMEM((halved, rows, cols), BF16)] + scratch,
        us=2,
    )(me, head_shift, *got[:halved])
    att = call(
        attention_body,
        sds((size_sp, tokens, cols), BF16),
        0,
        in_specs=[SM, SM] + [VM] * (2 + size_sp),
        scratch=[
            pltpu.VMEM((size_sp, rows, cols), BF16),
            pltpu.VMEM((size_sp, tokens, cols), F32),
            pltpu.VMEM((size_sp, local, tokens, tokens), F32),
        ]
        + scratch,
        us=6,
        limit=12,
    )(me, head_shift, *near, *got)
    att = lax.all_to_all(att, "sp", split_axis=0, concat_axis=0, tiled=True)
    row = lambda count: sds((count, width), BF16)
    hidden, *far = call(
        hidden_body, (row(tokens),) + (row(half),) * GROUPS, 6, us=2
    )(att, stream, mix_gain, out_weight, post_gain, dest_rows)
    for d in range(1, GROUPS):
        far[d] = swap(far[d], d * plane)

    def experts(pieces, takes, outs):
        if any(take % 8 for take in takes):
            pieces = [jnp.concatenate([p[:t] for p, t in zip(pieces, takes)], axis=0)]
            takes = [sum(takes)]
        return call(
            functools.partial(expert_body, takes=takes),
            tuple(row(o) for o in outs),
            len(takes) + 3,
            limit=8,
            us=0.02 * sum(takes),
        )(*pieces, w_gate, w_up, w_down)

    sums = [None] * GROUPS
    for chunk in CHUNKS:
        sources = len(chunk)
        block = row(CORES * cap * sources)
        part = cap * sources
        blocks = call(
            functools.partial(relay_body, sources=sources), (block,) * chips, 2 * sources
        )(*[far[d] for d in chunk], *[metas[d] for d in chunk])
        held = [blocks[0]] + [
            swap(blocks[m], CORES * m) for m in range(chips - 1, 0, -1)
        ][::-1]
        if part % 16:
            other = jnp.concatenate([b[part:] for b in held], axis=0)
        else:
            other = call(second_halves_body, row(chips * part), chips)(*held)
        other = swap(other, 1)
        own, reply = experts(
            held + [other], [part] * chips + [chips * part], [chips * part, chips * part]
        )
        back = swap(reply, 1)
        if part % 16:
            joined = [
                jnp.concatenate([a[m * part : (m + 1) * part] for a in (own, back)], axis=0)
                for m in range(chips)
            ]
        else:
            joined = call(join_body, (block,) * chips, 2)(own, back)
        got_back = [joined[0]] + [swap(joined[m], CORES * m) for m in range(chips - 1, 0, -1)][::-1]
        if block.shape[0] % 16:
            got_back = [jnp.concatenate(got_back, axis=0)]
        got_back = call(
            functools.partial(gather_body, sources=sources),
            (row(half),) * sources,
            sources + len(got_back),
        )(*[metas[d] for d in chunk], *got_back)
        for d, total in zip(chunk, got_back):
            sums[d] = swap(total, d * plane) if d else total
    partly = call(
        functools.partial(gathered_body, first=0), sds((tokens, width), F32), GROUPS + 1
    )(*sums[:-1], hidden, dest_cols)
    return call(
        functools.partial(gathered_body, first=GROUPS - 1), sds((1, tokens, width), BF16), 3
    )(sums[-1], partly, dest_cols)


def solution(mesh):
    return jax.shard_map(
        on_device,
        mesh=mesh,
        in_specs=(
            P("dp", "sp", None),
            P("dp", "sp", None),
            P("dp", "sp", None),
            P("dp", "sp", None),
            P("dp", "sp", None),
            P(),
            P(),
            P(),
            P(),
            P("dp", "sp", None),
            P("dp", "sp", None),
            P(("sp", "dp"), None, None),
            P(("sp", "dp"), None, None),
            P(("sp", "dp"), None, None),
        ),
        out_specs=P("dp", "sp", None),
        check_vma=False,
    )
```

time: 154 us -> 148 us (0.961)
  blocking collectives: 15.2 us -> 0 us
  starting transfers between devices: 46.7 us -> 60.9 us
  waiting for transfers between devices: 60 us -> 48.9 us
  local copies, waits for them, and re-layouts: 5.88 us -> 9 us
  Pallas kernels: 25.2 us -> 28.2 us
    all_to_all x1 -> x0, blocking collectives: 15.2 us -> none  [on_device(): att = lax.all_to_all(att, 'sp', split_axis=0, concat_axis=0, tiled=True)]
    ppermute x40 -> x45, waiting for transfers between devices: 60 us -> 48 us  [swap(): return lax.ppermute(array, both, [(i, i ^ bit) for i in range(n_expert)])]
    ppermute x40 -> x45, starting transfers between devices: 46.7 us -> 57.2 us  [swap(): return lax.ppermute(array, both, [(i, i ^ bit) for i in range(n_expert)])]
    all_to_all x0 -> x1, starting transfers between devices: none -> 3.65 us  [on_device(): att = lax.all_to_all(att, 'sp', split_axis=0, concat_axis=0, tiled=True)]
    unnamed x15 -> x14, local copies, waits for them, and re-layouts: 5.88 us -> 9 us
    pallas_call x4 -> x6, Pallas kernels: 13.6 us -> 16.6 us  [the longest x1 6.16 us: on_device(): call(attention_body, sds((size_sp, tokens, cols), BF16), 0, in_specs=[SM,...]
    pallas_call x3 -> x4, Pallas kernels: 7.14 us -> 7.44 us  [experts(): call(functools.partial(expert_body, takes=takes), tuple((row(o) for o in...]
  transfers between devices with their start and end apart: 40 -> 46, of which waited for: 17 -> 15; matrix products, arithmetic and copies ran while one was open for 1% -> 0% of each run, Pallas kernels for 7% -> 12%
where the time goes in v2:
time: 148 us; the launch traced here: 147 us
  starting transfers between devices  60.9 us (41%)
  waiting for transfers between devices  48.9 us (33%)
  Pallas kernels  28.2 us (19%)
  local copies, waits for them, and re-layouts  9 us (6%)
    ppermute x45, starting transfers between devices, swap(): return lax.ppermute(array, both, [(i, i ^ bit) for i in range(n_expert)])  57.2 us
    ppermute x45, waiting for transfers between devices, swap(): return lax.ppermute(array, both, [(i, i ^ bit) for i in range(n_expert)])  48 us
    unnamed x14, local copies, waits for them, and re-layouts  9 us
    pallas_call x4, Pallas kernels, experts(): call(functools.partial(expert_body, takes=takes), tuple((row(o) for o in...  7.44 us
    pallas_call x1, Pallas kernels, on_device(): call(attention_body, sds((size_sp, tokens, cols), BF16), 0, in_specs=[SM,...  6.16 us
    pallas_call x1, Pallas kernels, on_device(): call(fetch_body, tuple((sds(x.shape, x.dtype) for x in later)), 0, in_spe...  3.7 us
    all_to_all x1, starting transfers between devices, on_device(): att = lax.all_to_all(att, 'sp', split_axis=0, concat_axis=0, tiled=True)  3.65 us
  transfers between devices with their start and end apart: 46, of which 15 were waited for; matrix products, arithmetic and copies ran while one was open for 0% of the time, Pallas kernels for 12%

profile of v2, /device:TPU:0, one launch (start us, length us, event | category | flops | bytes accessed | tf_op | source)
XLA Modules:
  0.0 147.3 jit_solution(16613618077678231674)
XLA Ops:
  0.1 2.2 %shard_map.136 = (bf16[400,128]{1,0:T(8,128)(2,1)S(1)}, bf16[400,128]{1,0:T(8,128)(2,1)S(1)}, bf16[400,128]{1,0:T(8,128)(2,1)S(1)}, bf16[400,128]{1,0:T(8,128)(2...) custom-call(s32[2]{0:T(128)S(1)} %pad_add_fusion.me_ref, ...), custom_call_target="tpu_custom_call" | custom-call | flops 15000000 | bytes 3000000 | tf_op jit(solution)/shard_map/pallas_call | solution.py:430
  2.3 3.1 %collective-permute-start.1 = (bf16[400,128]{1,0:T(8,128)(2,1)S(1)}, bf16[400,128]{1,0:T(8,128)(2,1)S(1)}, u32[]{:S(2)}, u32[]{:S(2)}) collective-permute-start(bf16[400,128]{1,0:T(8,128)(2,1)S(1)} %get-tuple-element.70), channel_id=1, source_target_pairs={{0,4},{1,5},{2,6},{3,7},{4,0},{5,1},{6,2},{7,3},{8,12},{9,13},{10,... | collective-permute-start | bytes 307208 | tf_op jit(solution)/shard_map/ppermute | solution.py:423
  6.9 4.0 %collective-permute-start = (bf16[400,128]{1,0:T(8,128)(2,1)S(1)}, bf16[400,128]{1,0:T(8,128)(2,1)S(1)}, u32[]{:S(2)}, u32[]{:S(2)}) collective-permute-start(bf16[400,128]{1,0:T(8,128)(2,1)S(1)} %get-tuple-element.68), channel_id=1, source_target_pairs={{0,24},{1,25},{2,26},{3,27},{4,28},{5,29},{6,30},{7,31},{8,16},{9,... | collective-permute-start | bytes 307208 | tf_op jit(solution)/shard_map/ppermute | solution.py:423
  10.9 3.9 %collective-permute-start.5 = (bf16[400,128]{1,0:T(8,128)(2,1)S(1)}, bf16[400,128]{1,0:T(8,128)(2,1)S(1)}, u32[]{:S(2)}, u32[]{:S(2)}) collective-permute-start(bf16[400,128]{1,0:T(8,128)(2,1)S(1)} %get-tuple-element.76), channel_id=1, source_target_pairs={{0,20},{1,21},{2,22},{3,23},{4,16},{5,17},{6,18},{7,19},{8,28},{9,... | collective-permute-start | bytes 307208 | tf_op jit(solution)/shard_map/ppermute | solution.py:423
  15.5 2.8 %shard_map.137 = (f32[4,128,128]{2,1,0:T(8,128)S(1)}, f32[4,2,128,128]{3,2,1,0:T(8,128)S(1)}) custom-call(s32[2]{0:T(128)S(1)} %pad_add_fusion.me_ref, f32[16]{0:T(128)S(1)} %copy-done.6, bf16[400,128]{1,0:T(8,128)(2,1)S(1)} %get-tuple-element.69.refs_0_, bf16[400,128]{1,0:T(8,128)(2,1)S(1)} %collective-permute-done.1.refs_1_, ...), custom_call_target="tpu_custom_call" | custom-call | flops 30000000 | bytes 6000000 | tf_op jit(solution)/shard_map/pallas_call | solution.py:479
  18.3 6.8 %collective-permute-done.4.refs_4_.refs_1_.refs_0_ = bf16[400,128]{1,0:T(8,128)(2,1)S(1)} collective-permute-done((bf16[400,128]{1,0:T(8,128)(2,1)S(1)}, bf16[400,128]{1,0:T(8,128)(2,1)S(1)}, u32[]{:S(2)}, u32[]{:S(2)}) %collective-permute-start.4) | collective-permute-done | bytes 102432 | tf_op jit(solution)/shard_map/ppermute | solution.py:423
  25.1 2.6 %collective-permute-done.5.refs_5_ = bf16[400,128]{1,0:T(8,128)(2,1)S(1)} collective-permute-done((bf16[400,128]{1,0:T(8,128)(2,1)S(1)}, bf16[400,128]{1,0:T(8,128)(2,1)S(1)}, u32[]{:S(2)}, u32[]{:S(2)}) %collective-permute-start.5) | collective-permute-done | bytes 102432 | tf_op jit(solution)/shard_map/ppermute | solution.py:423
  27.7 6.2 %shard_map.138 = bf16[8,128,128]{2,1,0:T(8,128)(2,1)} custom-call(s32[2]{0:T(128)S(1)} %pad_add_fusion.me_ref, f32[16]{0:T(128)S(1)} %copy-done.6, f32[4,128,128]{2,1,0:T(8,128)S(1)} %get-tuple-element.73.near_ref, f32[4,2,128,128]{3,2,1,0:T(8,128)S(1)} %get-tuple-element.74.near_carry_ref, bf16[400,128]{1,0:T(8,128)(2,1)S(1)} %get-tuple-element.69.refs_0_, ...), custom_call_target="tpu_custom_call" | custom-call | flops 90000000 | bytes 18000000 | tf_op jit(solution)/shard_map/pallas_call | solution.py:487
  33.8 3.6 %all-to-all-start = ((bf16[8,128,128]{2,1,0:T(8,128)(2,1)}), bf16[8,128,128]{2,1,0:T(8,128)(2,1)S(1)}, u32[]{:S(2)}, u32[]{:S(2)}) async-start(bf16[8,128,128]{2,1,0:T(8,128)(2,1)} %shard_map.138), calls=%async_computation | async-start | bytes 524288 | tf_op jit(solution)/shard_map/all_to_all | solution.py:501
  37.5 3.7 %shard_map.139 = (bf16[1024,2048]{1,0:T(8,128)(2,1)S(1)}, bf16[1,128,2048]{2,1,0:T(8,128)(2,1)S(1)}, f32[1,1024]{1,0:T(1,128)S(1)}, f32[1,2048]{1,0:T(1,128)S(1)}, bf16[1,1024,2048]{2,1,0:T(8,128)(2,1)S(1)}) custom-call(bf16[1024,2048]{1,0:T(8,128)(2,1)} %refs_0_.1, bf16[1,128,2048]{2,1,0:T(8,128)(2,1)} %refs_1_.1, f32[1,1024]{1,0:T(1,128)} %bitcast.9, ...), custom_call_target="tpu_custom_call" | custom-call | flops 75000000 | bytes 15000000 | tf_op jit(solution)/shard_map/pallas_call | solution.py:465
  41.2 2.0 %copy-done.2 = bf16[1,1024,2048]{2,1,0:T(8,128)(2,1)} copy-done((bf16[1,1024,2048]{2,1,0:T(8,128)(2,1)}, bf16[1,1024,2048]{2,1,0:T(8,128)(2,1)S(1)}, u32[]{:S(2)}) %copy-start.2) | copy-done | bytes 4194328
  43.2 2.0 %copy-done.4 = bf16[1024,2048]{1,0:T(8,128)(2,1)} copy-done((bf16[1024,2048]{1,0:T(8,128)(2,1)}, bf16[1024,2048]{1,0:T(8,128)(2,1)S(1)}, u32[]{:S(2)}) %copy-start.4) | copy-done | bytes 4194328
  46.0 2.2 %copy-done.5 = bf16[1024,2048]{1,0:T(8,128)(2,1)S(1)} copy-done((bf16[1024,2048]{1,0:T(8,128)(2,1)S(1)}, bf16[1024,2048]{1,0:T(8,128)(2,1)}, u32[]{:S(2)}) %copy-start.5) | copy-done | bytes 4194328
  50.9 2.3 %collective-permute-start.35 = (bf16[64,2048]{1,0:T(8,128)(2,1)S(1)}, bf16[64,2048]{1,0:T(8,128)(2,1)S(1)}, u32[]{:S(2)}, u32[]{:S(2)}) collective-permute-start(bf16[64,2048]{1,0:T(8,128)(2,1)S(1)} %get-tuple-element.118), channel_id=1, source_target_pairs={{0,16},{1,17},{2,18},{3,19},{4,20},{5,21},{6,22},{7,23},{8,24},{9,... | collective-permute-start | bytes 786440 | tf_op jit(solution)/shard_map/ppermute | solution.py:423
  54.0 7.2 %collective-permute-done.25.refs_0_ = bf16[64,2048]{1,0:T(8,128)(2,1)S(1)} collective-permute-done((bf16[64,2048]{1,0:T(8,128)(2,1)S(1)}, bf16[64,2048]{1,0:T(8,128)(2,1)S(1)}, u32[]{:S(2)}, u32[]{:S(2)}) %collective-permute-start.25) | collective-permute-done | bytes 262176 | tf_op jit(solution)/shard_map/ppermute | solution.py:423
  65.1 7.2 %collective-permute-done.35.refs_0_ = bf16[64,2048]{1,0:T(8,128)(2,1)S(1)} collective-permute-done((bf16[64,2048]{1,0:T(8,128)(2,1)S(1)}, bf16[64,2048]{1,0:T(8,128)(2,1)S(1)}, u32[]{:S(2)}, u32[]{:S(2)}) %collective-permute-start.35) | collective-permute-done | bytes 262176 | tf_op jit(solution)/shard_map/ppermute | solution.py:423
  79.3 1.6 %collective-permute-start.19 = (bf16[32,2048]{1,0:T(8,128)(2,1)S(1)}, bf16[32,2048]{1,0:T(8,128)(2,1)S(1)}, u32[]{:S(2)}, u32[]{:S(2)}) collective-permute-start(bf16[32,2048]{1,0:T(8,128)(2,1)S(1)} %get-tuple-element.100), channel_id=1, source_target_pairs={{0,6},{1,7},{2,4},{3,5},{4,2},{5,3},{6,0},{7,1},{8,14},{9,15},{10,... | collective-permute-start | bytes 393224 | tf_op jit(solution)/shard_map/ppermute | solution.py:423
  85.2 1.6 %collective-permute-start.10 = (bf16[32,2048]{1,0:T(8,128)(2,1)S(1)}, bf16[32,2048]{1,0:T(8,128)(2,1)S(1)}, u32[]{:S(2)}, u32[]{:S(2)}) collective-permute-start(bf16[32,2048]{1,0:T(8,128)(2,1)S(1)} %get-tuple-element.87), channel_id=1, source_target_pairs={{0,6},{1,7},{2,4},{3,5},{4,2},{5,3},{6,0},{7,1},{8,14},{9,15},{10,... | collective-permute-start | bytes 393224 | tf_op jit(solution)/shard_map/ppermute | solution.py:423
  86.9 2.7 %collective-permute-done.9.refs_2_ = bf16[32,2048]{1,0:T(8,128)(2,1)S(1)} collective-permute-done((bf16[32,2048]{1,0:T(8,128)(2,1)S(1)}, bf16[32,2048]{1,0:T(8,128)(2,1)S(1)}, u32[]{:S(2)}, u32[]{:S(2)}) %collective-permute-start.9) | collective-permute-done | bytes 131104 | tf_op jit(solution)/shard_map/ppermute | solution.py:423
  91.2 2.2 %copy-done.3 = bf16[1,1024,2048]{2,1,0:T(8,128)(2,1)S(1)} copy-done((bf16[1,1024,2048]{2,1,0:T(8,128)(2,1)S(1)}, bf16[1,1024,2048]{2,1,0:T(8,128)(2,1)}, u32[]{:S(2)}) %copy-start.3) | copy-done | bytes 4194328
  93.4 1.9 %shard_map.153 = (bf16[64,2048]{1,0:T(8,128)(2,1)S(1)}, bf16[64,2048]{1,0:T(8,128)(2,1)S(1)}) custom-call(bf16[32,2048]{1,0:T(8,128)(2,1)S(1)} %get-tuple-element.108.refs_0_, bf16[32,2048]{1,0:T(8,128)(2,1)S(1)} %collective-permute-done.26.refs_1_, bf16[32,2048]{1,0:T(8,128)(2,1)S(1)} %collective-permute-done.27.refs_2_, ...), custom_call_target="tpu_custom_call" | custom-call | flops 38400000 | bytes 7680000 | tf_op jit(solution)/shard_map/pallas_call | solution.py:513
  95.8 1.9 %shard_map.158 = (bf16[64,2048]{1,0:T(8,128)(2,1)S(1)}, bf16[64,2048]{1,0:T(8,128)(2,1)S(1)}) custom-call(bf16[32,2048]{1,0:T(8,128)(2,1)S(1)} %get-tuple-element.119.refs_0_, bf16[32,2048]{1,0:T(8,128)(2,1)S(1)} %collective-permute-done.36.refs_1_, bf16[32,2048]{1,0:T(8,128)(2,1)S(1)} %collective-permute-done.37.refs_2_, ...), custom_call_target="tpu_custom_call" | custom-call | flops 38400000 | bytes 7680000 | tf_op jit(solution)/shard_map/pallas_call | solution.py:513
  97.7 1.9 %shard_map.148 = (bf16[64,2048]{1,0:T(8,128)(2,1)S(1)}, bf16[64,2048]{1,0:T(8,128)(2,1)S(1)}) custom-call(bf16[32,2048]{1,0:T(8,128)(2,1)S(1)} %get-tuple-element.97.refs_0_, bf16[32,2048]{1,0:T(8,128)(2,1)S(1)} %collective-permute-done.17.refs_1_, bf16[32,2048]{1,0:T(8,128)(2,1)S(1)} %collective-permute-done.18.refs_2_, ...), custom_call_target="tpu_custom_call" | custom-call | flops 38400000 | bytes 7680000 | tf_op jit(solution)/shard_map/pallas_call | solution.py:513
  100.1 1.9 %shard_map.143 = (bf16[64,2048]{1,0:T(8,128)(2,1)S(1)}, bf16[64,2048]{1,0:T(8,128)(2,1)S(1)}) custom-call(bf16[32,2048]{1,0:T(8,128)(2,1)S(1)} %get-tuple-element.84.refs_0_, bf16[32,2048]{1,0:T(8,128)(2,1)S(1)} %collective-permute-done.8.refs_1_, bf16[32,2048]{1,0:T(8,128)(2,1)S(1)} %collective-permute-done.9.refs_2_, ...), custom_call_target="tpu_custom_call" | custom-call | flops 38400000 | bytes 7680000 | tf_op jit(solution)/shard_map/pallas_call | solution.py:513
  108.6 1.6 %collective-permute-start.43 = (bf16[32,2048]{1,0:T(8,128)(2,1)S(1)}, bf16[32,2048]{1,0:T(8,128)(2,1)S(1)}, u32[]{:S(2)}, u32[]{:S(2)}) collective-permute-start(bf16[32,2048]{1,0:T(8,128)(2,1)S(1)} %get-tuple-element.128), channel_id=1, source_target_pairs={{0,6},{1,7},{2,4},{3,5},{4,2},{5,3},{6,0},{7,1},{8,14},{9,15},{10,... | collective-permute-start | bytes 393224 | tf_op jit(solution)/shard_map/ppermute | solution.py:423
  110.2 2.1 %collective-permute-done.32.refs_3_ = bf16[32,2048]{1,0:T(8,128)(2,1)S(1)} collective-permute-done((bf16[32,2048]{1,0:T(8,128)(2,1)S(1)}, bf16[32,2048]{1,0:T(8,128)(2,1)S(1)}, u32[]{:S(2)}, u32[]{:S(2)}) %collective-permute-start.32) | collective-permute-done | bytes 131104 | tf_op jit(solution)/shard_map/ppermute | solution.py:423
  114.3 1.6 %collective-permute-start.15 = (bf16[32,2048]{1,0:T(8,128)(2,1)S(1)}, bf16[32,2048]{1,0:T(8,128)(2,1)S(1)}, u32[]{:S(2)}, u32[]{:S(2)}) collective-permute-start(bf16[32,2048]{1,0:T(8,128)(2,1)S(1)} %get-tuple-element.94), channel_id=1, source_target_pairs={{0,6},{1,7},{2,4},{3,5},{4,2},{5,3},{6,0},{7,1},{8,14},{9,15},{10,... | collective-permute-start | bytes 393224 | tf_op jit(solution)/shard_map/ppermute | solution.py:423
  116.3 1.7 %collective-permute-done.42.refs_3_ = bf16[32,2048]{1,0:T(8,128)(2,1)S(1)} collective-permute-done((bf16[32,2048]{1,0:T(8,128)(2,1)S(1)}, bf16[32,2048]{1,0:T(8,128)(2,1)S(1)}, u32[]{:S(2)}, u32[]{:S(2)}) %collective-permute-start.42) | collective-permute-done | bytes 131104 | tf_op jit(solution)/shard_map/ppermute | solution.py:423
  118.5 6.2 %collective-permute-start.34 = (bf16[64,2048]{1,0:T(8,128)(2,1)S(1)}, bf16[64,2048]{1,0:T(8,128)(2,1)S(1)}, u32[]{:S(2)}, u32[]{:S(2)}) collective-permute-start(bf16[64,2048]{1,0:T(8,128)(2,1)S(1)} %shard_map.155), channel_id=1, source_target_pairs={{0,8},{1,9},{2,10},{3,11},{4,12},{5,13},{6,14},{7,15},{8,0},{9,1},... | collective-permute-start | bytes 786440 | tf_op jit(solution)/shard_map/ppermute | solution.py:423
  126.2 2.4 %collective-permute-start.16 = (bf16[64,2048]{1,0:T(8,128)(2,1)S(1)}, bf16[64,2048]{1,0:T(8,128)(2,1)S(1)}, u32[]{:S(2)}, u32[]{:S(2)}) collective-permute-start(bf16[64,2048]{1,0:T(8,128)(2,1)S(1)} %shard_map.145), channel_id=1, source_target_pairs={{0,24},{1,25},{2,26},{3,27},{4,28},{5,29},{6,30},{7,31},{8,16},{9,... | collective-permute-start | bytes 786440 | tf_op jit(solution)/shard_map/ppermute | solution.py:423
  131.0 4.8 %collective-permute-done.23.refs_3_ = bf16[32,2048]{1,0:T(8,128)(2,1)S(1)} collective-permute-done((bf16[32,2048]{1,0:T(8,128)(2,1)S(1)}, bf16[32,2048]{1,0:T(8,128)(2,1)S(1)}, u32[]{:S(2)}, u32[]{:S(2)}) %collective-permute-start.23) | collective-permute-done | bytes 131104 | tf_op jit(solution)/shard_map/ppermute | solution.py:423
  136.1 9.5 %collective-permute-done.44.refs_2_ = bf16[64,2048]{1,0:T(8,128)(2,1)S(1)} collective-permute-done((bf16[64,2048]{1,0:T(8,128)(2,1)S(1)}, bf16[64,2048]{1,0:T(8,128)(2,1)S(1)}, u32[]{:S(2)}, u32[]{:S(2)}) %collective-permute-start.44) | collective-permute-done | bytes 262176 | tf_op jit(solution)/shard_map/ppermute | solution.py:423
  (102 shorter events, 39.9 us)
Async XLA Ops:
  2.3 8.6 %collective-permute-start.1 = (bf16[400,128]{1,0:T(8,128)(2,1)S(1)}, bf16[400,128]{1,0:T(8,128)(2,1)S(1)}, u32[]{:S(2)}, u32[]{:S(2)}) collective-permute-start(bf16[400,128]{1,0:T(8,128)(2,1)S(1)} %get-tuple-element.70), channel_id=1, source_target_pairs={{0,4},{1,5},{2,6},{3,7},{4,0},{5,1},{6,2},{7,3},{8,12},{9,13},{10,... | collective-permute-start | bytes 307208 | tf_op jit(solution)/shard_map/ppermute | solution.py:423
  5.4 9.5 %collective-permute-start.2 = (bf16[400,128]{1,0:T(8,128)(2,1)S(1)}, bf16[400,128]{1,0:T(8,128)(2,1)S(1)}, u32[]{:S(2)}, u32[]{:S(2)}) collective-permute-start(bf16[400,128]{1,0:T(8,128)(2,1)S(1)} %get-tuple-element.71), channel_id=1, source_target_pairs={{0,8},{1,9},{2,10},{3,11},{4,12},{5,13},{6,14},{7,15},{8,0},{9,1},... | collective-permute-start | bytes 307208 | tf_op jit(solution)/shard_map/ppermute | solution.py:423
  6.9 7.9 %collective-permute-start.3 = (bf16[400,128]{1,0:T(8,128)(2,1)S(1)}, bf16[400,128]{1,0:T(8,128)(2,1)S(1)}, u32[]{:S(2)}, u32[]{:S(2)}) collective-permute-start(bf16[400,128]{1,0:T(8,128)(2,1)S(1)} %get-tuple-element.72), channel_id=1, source_target_pairs={{0,12},{1,13},{2,14},{3,15},{4,8},{5,9},{6,10},{7,11},{8,4},{9,5},... | collective-permute-start | bytes 307208 | tf_op jit(solution)/shard_map/ppermute | solution.py:423
  6.9 11.3 %collective-permute-start = (bf16[400,128]{1,0:T(8,128)(2,1)S(1)}, bf16[400,128]{1,0:T(8,128)(2,1)S(1)}, u32[]{:S(2)}, u32[]{:S(2)}) collective-permute-start(bf16[400,128]{1,0:T(8,128)(2,1)S(1)} %get-tuple-element.68), channel_id=1, source_target_pairs={{0,24},{1,25},{2,26},{3,27},{4,28},{5,29},{6,30},{7,31},{8,16},{9,... | collective-permute-start | bytes 307208 | tf_op jit(solution)/shard_map/ppermute | solution.py:423
  10.9 14.2 %collective-permute-start.4 = (bf16[400,128]{1,0:T(8,128)(2,1)S(1)}, bf16[400,128]{1,0:T(8,128)(2,1)S(1)}, u32[]{:S(2)}, u32[]{:S(2)}) collective-permute-start(bf16[400,128]{1,0:T(8,128)(2,1)S(1)} %get-tuple-element.75), channel_id=1, source_target_pairs={{0,16},{1,17},{2,18},{3,19},{4,20},{5,21},{6,22},{7,23},{8,24},{9,... | collective-permute-start | bytes 307208 | tf_op jit(solution)/shard_map/ppermute | solution.py:423
  10.9 16.7 %collective-permute-start.5 = (bf16[400,128]{1,0:T(8,128)(2,1)S(1)}, bf16[400,128]{1,0:T(8,128)(2,1)S(1)}, u32[]{:S(2)}, u32[]{:S(2)}) collective-permute-start(bf16[400,128]{1,0:T(8,128)(2,1)S(1)} %get-tuple-element.76), channel_id=1, source_target_pairs={{0,20},{1,21},{2,22},{3,23},{4,16},{5,17},{6,18},{7,19},{8,28},{9,... | collective-permute-start | bytes 307208 | tf_op jit(solution)/shard_map/ppermute | solution.py:423
  14.8 12.8 %collective-permute-start.6 = (bf16[400,128]{1,0:T(8,128)(2,1)S(1)}, bf16[400,128]{1,0:T(8,128)(2,1)S(1)}, u32[]{:S(2)}, u32[]{:S(2)}) collective-permute-start(bf16[400,128]{1,0:T(8,128)(2,1)S(1)} %get-tuple-element.77), channel_id=1, source_target_pairs={{0,28},{1,29},{2,30},{3,31},{4,24},{5,25},{6,26},{7,27},{8,20},{9,... | collective-permute-start | bytes 307208 | tf_op jit(solution)/shard_map/ppermute | solution.py:423
  33.8 12.2 %all-to-all-start = ((bf16[8,128,128]{2,1,0:T(8,128)(2,1)}), bf16[8,128,128]{2,1,0:T(8,128)(2,1)S(1)}, u32[]{:S(2)}, u32[]{:S(2)}) async-start(bf16[8,128,128]{2,1,0:T(8,128)(2,1)} %shard_map.138), calls=%async_computation | async-start | bytes 524288 | tf_op jit(solution)/shard_map/all_to_all | solution.py:501
  49.6 11.7 %collective-permute-start.25 = (bf16[64,2048]{1,0:T(8,128)(2,1)S(1)}, bf16[64,2048]{1,0:T(8,128)(2,1)S(1)}, u32[]{:S(2)}, u32[]{:S(2)}) collective-permute-start(bf16[64,2048]{1,0:T(8,128)(2,1)S(1)} %get-tuple-element.107), channel_id=1, source_target_pairs={{0,8},{1,9},{2,10},{3,11},{4,12},{5,13},{6,14},{7,15},{8,0},{9,1},... | collective-permute-start | bytes 786440 | tf_op jit(solution)/shard_map/ppermute | solution.py:423
  50.9 21.3 %collective-permute-start.35 = (bf16[64,2048]{1,0:T(8,128)(2,1)S(1)}, bf16[64,2048]{1,0:T(8,128)(2,1)S(1)}, u32[]{:S(2)}, u32[]{:S(2)}) collective-permute-start(bf16[64,2048]{1,0:T(8,128)(2,1)S(1)} %get-tuple-element.118), channel_id=1, source_target_pairs={{0,16},{1,17},{2,18},{3,19},{4,20},{5,21},{6,22},{7,23},{8,24},{9,... | collective-permute-start | bytes 786440 | tf_op jit(solution)/shard_map/ppermute | solution.py:423
  53.2 20.9 %collective-permute-start.7 = (bf16[64,2048]{1,0:T(8,128)(2,1)S(1)}, bf16[64,2048]{1,0:T(8,128)(2,1)S(1)}, u32[]{:S(2)}, u32[]{:S(2)}) collective-permute-start(bf16[64,2048]{1,0:T(8,128)(2,1)S(1)} %get-tuple-element.83), channel_id=1, source_target_pairs={{0,24},{1,25},{2,26},{3,27},{4,28},{5,29},{6,30},{7,31},{8,16},{9,... | collective-permute-start | bytes 786440 | tf_op jit(solution)/shard_map/ppermute | solution.py:423
  61.5 13.9 %collective-permute-start.26 = (bf16[32,2048]{1,0:T(8,128)(2,1)S(1)}, bf16[32,2048]{1,0:T(8,128)(2,1)S(1)}, u32[]{:S(2)}, u32[]{:S(2)}) collective-permute-start(bf16[32,2048]{1,0:T(8,128)(2,1)S(1)} %get-tuple-element.109), channel_id=1, source_target_pairs={{0,2},{1,3},{2,0},{3,1},{4,6},{5,7},{6,4},{7,5},{8,10},{9,11},{10,... | collective-permute-start | bytes 393224 | tf_op jit(solution)/shard_map/ppermute | solution.py:423
  63.1 13.3 %collective-permute-start.27 = (bf16[32,2048]{1,0:T(8,128)(2,1)S(1)}, bf16[32,2048]{1,0:T(8,128)(2,1)S(1)}, u32[]{:S(2)}, u32[]{:S(2)}) collective-permute-start(bf16[32,2048]{1,0:T(8,128)(2,1)S(1)} %get-tuple-element.110), channel_id=1, source_target_pairs={{0,4},{1,5},{2,6},{3,7},{4,0},{5,1},{6,2},{7,3},{8,12},{9,13},{10,... | collective-permute-start | bytes 393224 | tf_op jit(solution)/shard_map/ppermute | solution.py:423
  64.1 13.9 %collective-permute-start.28 = (bf16[32,2048]{1,0:T(8,128)(2,1)S(1)}, bf16[32,2048]{1,0:T(8,128)(2,1)S(1)}, u32[]{:S(2)}, u32[]{:S(2)}) collective-permute-start(bf16[32,2048]{1,0:T(8,128)(2,1)S(1)} %get-tuple-element.111), channel_id=1, source_target_pairs={{0,6},{1,7},{2,4},{3,5},{4,2},{5,3},{6,0},{7,1},{8,14},{9,15},{10,... | collective-permute-start | bytes 393224 | tf_op jit(solution)/shard_map/ppermute | solution.py:423
  74.1 7.1 %collective-permute-start.37 = (bf16[32,2048]{1,0:T(8,128)(2,1)S(1)}, bf16[32,2048]{1,0:T(8,128)(2,1)S(1)}, u32[]{:S(2)}, u32[]{:S(2)}) collective-permute-start(bf16[32,2048]{1,0:T(8,128)(2,1)S(1)} %get-tuple-element.121), channel_id=1, source_target_pairs={{0,4},{1,5},{2,6},{3,7},{4,0},{5,1},{6,2},{7,3},{8,12},{9,13},{10,... | collective-permute-start | bytes 393224 | tf_op jit(solution)/shard_map/ppermute | solution.py:423
  82.0 9.1 %collective-permute-start.29 = (bf16[64,2048]{1,0:T(8,128)(2,1)S(1)}, bf16[64,2048]{1,0:T(8,128)(2,1)S(1)}, u32[]{:S(2)}, u32[]{:S(2)}) collective-permute-start(bf16[64,2048]{1,0:T(8,128)(2,1)S(1)} %shard_map.152), channel_id=1, source_target_pairs={{0,1},{1,0},{2,3},{3,2},{4,5},{5,4},{6,7},{7,6},{8,9},{9,8},{10,11... | collective-permute-start | bytes 786440 | tf_op jit(solution)/shard_map/ppermute | solution.py:423
  82.1 13.7 %collective-permute-start.39 = (bf16[64,2048]{1,0:T(8,128)(2,1)S(1)}, bf16[64,2048]{1,0:T(8,128)(2,1)S(1)}, u32[]{:S(2)}, u32[]{:S(2)}) collective-permute-start(bf16[64,2048]{1,0:T(8,128)(2,1)S(1)} %shard_map.157), channel_id=1, source_target_pairs={{0,1},{1,0},{2,3},{3,2},{4,5},{5,4},{6,7},{7,6},{8,9},{9,8},{10,11... | collective-permute-start | bytes 786440 | tf_op jit(solution)/shard_map/ppermute | solution.py:423
  86.8 10.9 %collective-permute-start.20 = (bf16[64,2048]{1,0:T(8,128)(2,1)S(1)}, bf16[64,2048]{1,0:T(8,128)(2,1)S(1)}, u32[]{:S(2)}, u32[]{:S(2)}) collective-permute-start(bf16[64,2048]{1,0:T(8,128)(2,1)S(1)} %shard_map.147), channel_id=1, source_target_pairs={{0,1},{1,0},{2,3},{3,2},{4,5},{5,4},{6,7},{7,6},{8,9},{9,8},{10,11... | collective-permute-start | bytes 786440 | tf_op jit(solution)/shard_map/ppermute | solution.py:423
  91.1 9.1 %collective-permute-start.11 = (bf16[64,2048]{1,0:T(8,128)(2,1)S(1)}, bf16[64,2048]{1,0:T(8,128)(2,1)S(1)}, u32[]{:S(2)}, u32[]{:S(2)}) collective-permute-start(bf16[64,2048]{1,0:T(8,128)(2,1)S(1)} %shard_map.142), channel_id=1, source_target_pairs={{0,1},{1,0},{2,3},{3,2},{4,5},{5,4},{6,7},{7,6},{8,9},{9,8},{10,11... | collective-permute-start | bytes 786440 | tf_op jit(solution)/shard_map/ppermute | solution.py:423
  103.5 8.9 %collective-permute-start.32 = (bf16[32,2048]{1,0:T(8,128)(2,1)S(1)}, bf16[32,2048]{1,0:T(8,128)(2,1)S(1)}, u32[]{:S(2)}, u32[]{:S(2)}) collective-permute-start(bf16[32,2048]{1,0:T(8,128)(2,1)S(1)} %get-tuple-element.116), channel_id=1, source_target_pairs={{0,4},{1,5},{2,6},{3,7},{4,0},{5,1},{6,2},{7,3},{8,12},{9,13},{10,... | collective-permute-start | bytes 393224 | tf_op jit(solution)/shard_map/ppermute | solution.py:423
  104.4 8.5 %collective-permute-start.33 = (bf16[32,2048]{1,0:T(8,128)(2,1)S(1)}, bf16[32,2048]{1,0:T(8,128)(2,1)S(1)}, u32[]{:S(2)}, u32[]{:S(2)}) collective-permute-start(bf16[32,2048]{1,0:T(8,128)(2,1)S(1)} %get-tuple-element.117), channel_id=1, source_target_pairs={{0,6},{1,7},{2,4},{3,5},{4,2},{5,3},{6,0},{7,1},{8,14},{9,15},{10,... | collective-permute-start | bytes 393224 | tf_op jit(solution)/shard_map/ppermute | solution.py:423
  105.8 8.5 %collective-permute-start.41 = (bf16[32,2048]{1,0:T(8,128)(2,1)S(1)}, bf16[32,2048]{1,0:T(8,128)(2,1)S(1)}, u32[]{:S(2)}, u32[]{:S(2)}) collective-permute-start(bf16[32,2048]{1,0:T(8,128)(2,1)S(1)} %get-tuple-element.126), channel_id=1, source_target_pairs={{0,2},{1,3},{2,0},{3,1},{4,6},{5,7},{6,4},{7,5},{8,10},{9,11},{10,... | collective-permute-start | bytes 393224 | tf_op jit(solution)/shard_map/ppermute | solution.py:423
  107.1 10.9 %collective-permute-start.42 = (bf16[32,2048]{1,0:T(8,128)(2,1)S(1)}, bf16[32,2048]{1,0:T(8,128)(2,1)S(1)}, u32[]{:S(2)}, u32[]{:S(2)}) collective-permute-start(bf16[32,2048]{1,0:T(8,128)(2,1)S(1)} %get-tuple-element.127), channel_id=1, source_target_pairs={{0,4},{1,5},{2,6},{3,7},{4,0},{5,1},{6,2},{7,3},{8,12},{9,13},{10,... | collective-permute-start | bytes 393224 | tf_op jit(solution)/shard_map/ppermute | solution.py:423
  108.6 9.9 %collective-permute-start.43 = (bf16[32,2048]{1,0:T(8,128)(2,1)S(1)}, bf16[32,2048]{1,0:T(8,128)(2,1)S(1)}, u32[]{:S(2)}, u32[]{:S(2)}) collective-permute-start(bf16[32,2048]{1,0:T(8,128)(2,1)S(1)} %get-tuple-element.128), channel_id=1, source_target_pairs={{0,6},{1,7},{2,4},{3,5},{4,2},{5,3},{6,0},{7,1},{8,14},{9,15},{10,... | collective-permute-start | bytes 393224 | tf_op jit(solution)/shard_map/ppermute | solution.py:423
  112.4 12.7 %collective-permute-start.13 = (bf16[32,2048]{1,0:T(8,128)(2,1)S(1)}, bf16[32,2048]{1,0:T(8,128)(2,1)S(1)}, u32[]{:S(2)}, u32[]{:S(2)}) collective-permute-start(bf16[32,2048]{1,0:T(8,128)(2,1)S(1)} %get-tuple-element.92), channel_id=1, source_target_pairs={{0,2},{1,3},{2,0},{3,1},{4,6},{5,7},{6,4},{7,5},{8,10},{9,11},{10,... | collective-permute-start | bytes 393224 | tf_op jit(solution)/shard_map/ppermute | solution.py:423
  112.9 12.9 %collective-permute-start.14 = (bf16[32,2048]{1,0:T(8,128)(2,1)S(1)}, bf16[32,2048]{1,0:T(8,128)(2,1)S(1)}, u32[]{:S(2)}, u32[]{:S(2)}) collective-permute-start(bf16[32,2048]{1,0:T(8,128)(2,1)S(1)} %get-tuple-element.93), channel_id=1, source_target_pairs={{0,4},{1,5},{2,6},{3,7},{4,0},{5,1},{6,2},{7,3},{8,12},{9,13},{10,... | collective-permute-start | bytes 393224 | tf_op jit(solution)/shard_map/ppermute | solution.py:423
  114.3 11.5 %collective-permute-start.15 = (bf16[32,2048]{1,0:T(8,128)(2,1)S(1)}, bf16[32,2048]{1,0:T(8,128)(2,1)S(1)}, u32[]{:S(2)}, u32[]{:S(2)}) collective-permute-start(bf16[32,2048]{1,0:T(8,128)(2,1)S(1)} %get-tuple-element.94), channel_id=1, source_target_pairs={{0,6},{1,7},{2,4},{3,5},{4,2},{5,3},{6,0},{7,1},{8,14},{9,15},{10,... | collective-permute-start | bytes 393224 | tf_op jit(solution)/shard_map/ppermute | solution.py:423
  118.0 11.7 %collective-permute-start.22 = (bf16[32,2048]{1,0:T(8,128)(2,1)S(1)}, bf16[32,2048]{1,0:T(8,128)(2,1)S(1)}, u32[]{:S(2)}, u32[]{:S(2)}) collective-permute-start(bf16[32,2048]{1,0:T(8,128)(2,1)S(1)} %get-tuple-element.104), channel_id=1, source_target_pairs={{0,2},{1,3},{2,0},{3,1},{4,6},{5,7},{6,4},{7,5},{8,10},{9,11},{10,... | collective-permute-start | bytes 393224 | tf_op jit(solution)/shard_map/ppermute | solution.py:423
  118.5 17.6 %collective-permute-start.34 = (bf16[64,2048]{1,0:T(8,128)(2,1)S(1)}, bf16[64,2048]{1,0:T(8,128)(2,1)S(1)}, u32[]{:S(2)}, u32[]{:S(2)}) collective-permute-start(bf16[64,2048]{1,0:T(8,128)(2,1)S(1)} %shard_map.155), channel_id=1, source_target_pairs={{0,8},{1,9},{2,10},{3,11},{4,12},{5,13},{6,14},{7,15},{8,0},{9,1},... | collective-permute-start | bytes 786440 | tf_op jit(solution)/shard_map/ppermute | solution.py:423
  125.1 20.5 %collective-permute-start.44 = (bf16[64,2048]{1,0:T(8,128)(2,1)S(1)}, bf16[64,2048]{1,0:T(8,128)(2,1)S(1)}, u32[]{:S(2)}, u32[]{:S(2)}) collective-permute-start(bf16[64,2048]{1,0:T(8,128)(2,1)S(1)} %shard_map.160), channel_id=1, source_target_pairs={{0,16},{1,17},{2,18},{3,19},{4,20},{5,21},{6,22},{7,23},{8,24},{9,... | collective-permute-start | bytes 786440 | tf_op jit(solution)/shard_map/ppermute | solution.py:423
  126.2 20.0 %collective-permute-start.16 = (bf16[64,2048]{1,0:T(8,128)(2,1)S(1)}, bf16[64,2048]{1,0:T(8,128)(2,1)S(1)}, u32[]{:S(2)}, u32[]{:S(2)}) collective-permute-start(bf16[64,2048]{1,0:T(8,128)(2,1)S(1)} %shard_map.145), channel_id=1, source_target_pairs={{0,24},{1,25},{2,26},{3,27},{4,28},{5,29},{6,30},{7,31},{8,16},{9,... | collective-permute-start | bytes 786440 | tf_op jit(solution)/shard_map/ppermute | solution.py:423
  128.6 7.1 %collective-permute-start.23 = (bf16[32,2048]{1,0:T(8,128)(2,1)S(1)}, bf16[32,2048]{1,0:T(8,128)(2,1)S(1)}, u32[]{:S(2)}, u32[]{:S(2)}) collective-permute-start(bf16[32,2048]{1,0:T(8,128)(2,1)S(1)} %get-tuple-element.105), channel_id=1, source_target_pairs={{0,4},{1,5},{2,6},{3,7},{4,0},{5,1},{6,2},{7,3},{8,12},{9,13},{10,... | collective-permute-start | bytes 393224 | tf_op jit(solution)/shard_map/ppermute | solution.py:423
  (21 other events, 180.3 us)

commit v3 on v2

--- a/solution.py
+++ b/solution.py
@@ -12,6 +12,7 @@
 HD = 64
 GROUPS = 4
 CORES = 2
+EARLY, LATE = (0, 2), (1, 3)
 CHUNKS = ((2,), (3,), (1,), (0,))
 norm_eps = 1e-05
 F32 = jnp.float32
@@ -376,11 +377,11 @@
         out_ref[...] = total.astype(BF16)
 
 
-def gathered_body(*refs, first):
+def gathered_body(*refs, chosen):
     far_refs, (hid_ref, dest_ref, out_ref) = refs[:-3], refs[-3:]
     tokens = hid_ref.shape[0]
     result = hid_ref[...].astype(F32)
-    for d, ref in enumerate(far_refs, first):
+    for d, ref in zip(chosen, far_refs):
         slot = iota((tokens, ref.shape[0]), 1)
         hot = (slot == dest_ref[:, d : d + 1]).astype(F32).astype(BF16)
         result = result + jnp.dot(hot, ref[...], preferred_element_type=F32)
@@ -556,11 +557,11 @@
         for d, total in zip(chunk, got_back):
             sums[d] = swap(total, d * plane) if d else total
     partly = call(
-        functools.partial(gathered_body, first=0), sds((tokens, width), F32), GROUPS + 1
-    )(*sums[:-1], hidden, dest_cols)
+        functools.partial(gathered_body, chosen=EARLY), sds((tokens, width), F32), len(EARLY) + 2
+    )(*[sums[d] for d in EARLY], hidden, dest_cols)
     return call(
-        functools.partial(gathered_body, first=GROUPS - 1), sds((1, tokens, width), BF16), 3
-    )(sums[-1], partly, dest_cols)
+        functools.partial(gathered_body, chosen=LATE), sds((1, tokens, width), BF16), len(LATE) + 2
+    )(*[sums[d] for d in LATE], partly, dest_cols)
 
 
 def solution(mesh):

time: 148 us -> 148 us (level)
  waiting for transfers between devices: 48.9 us -> 47.1 us
  starting transfers between devices: 60.9 us -> 62.6 us
    all_to_all x1, starting transfers between devices: 3.65 us -> 6.56 us  [on_device(): att = lax.all_to_all(att, 'sp', split_axis=0, concat_axis=0, tiled=True)]
    ppermute x45, waiting for transfers between devices: 48 us -> 46.3 us  [swap(): return lax.ppermute(array, both, [(i, i ^ bit) for i in range(n_expert)])]
  transfers between devices with their start and end apart: 46 -> 46, of which waited for: 15 -> 13; matrix products, arithmetic and copies ran while one was open for 0% -> 0% of each run, Pallas kernels for 12% -> 12%
where the time goes in v3:
time: 148 us; the launch traced here: 147 us
  starting transfers between devices  62.6 us (42%)
  waiting for transfers between devices  47.1 us (32%)
  Pallas kernels  28.2 us (19%)
  local copies, waits for them, and re-layouts  9.01 us (6%)
    ppermute x45, starting transfers between devices, swap(): return lax.ppermute(array, both, [(i, i ^ bit) for i in range(n_expert)])  56.1 us
    ppermute x45, waiting for transfers between devices, swap(): return lax.ppermute(array, both, [(i, i ^ bit) for i in range(n_expert)])  46.3 us
    unnamed x14, local copies, waits for them, and re-layouts  9.01 us
    pallas_call x4, Pallas kernels, experts(): call(functools.partial(expert_body, takes=takes), tuple((row(o) for o in...  7.44 us
    all_to_all x1, starting transfers between devices, on_device(): att = lax.all_to_all(att, 'sp', split_axis=0, concat_axis=0, tiled=True)  6.56 us
    pallas_call x1, Pallas kernels, on_device(): call(attention_body, sds((size_sp, tokens, cols), BF16), 0, in_specs=[SM,...  6.17 us
    pallas_call x1, Pallas kernels, on_device(): call(fetch_body, tuple((sds(x.shape, x.dtype) for x in later)), 0, in_spe...  3.7 us
  transfers between devices with their start and end apart: 46, of which 13 were waited for; matrix products, arithmetic and copies ran while one was open for 0% of the time, Pallas kernels for 12%

profile of v3, /device:TPU:0, one launch (start us, length us, event | category | flops | bytes accessed | tf_op | source)
XLA Modules:
  0.0 147.3 jit_solution(14383957456186901682)
XLA Ops:
  0.1 2.2 %shard_map.136 = (bf16[400,128]{1,0:T(8,128)(2,1)S(1)}, bf16[400,128]{1,0:T(8,128)(2,1)S(1)}, bf16[400,128]{1,0:T(8,128)(2,1)S(1)}, bf16[400,128]{1,0:T(8,128)(2...) custom-call(s32[2]{0:T(128)S(1)} %pad_add_fusion.me_ref, ...), custom_call_target="tpu_custom_call" | custom-call | flops 15000000 | bytes 3000000 | tf_op jit(solution)/shard_map/pallas_call | solution.py:431
  2.3 3.1 %collective-permute-start = (bf16[400,128]{1,0:T(8,128)(2,1)S(1)}, bf16[400,128]{1,0:T(8,128)(2,1)S(1)}, u32[]{:S(2)}, u32[]{:S(2)}) collective-permute-start(bf16[400,128]{1,0:T(8,128)(2,1)S(1)} %get-tuple-element.68), channel_id=1, source_target_pairs={{0,8},{1,9},{2,10},{3,11},{4,12},{5,13},{6,14},{7,15},{8,0},{9,1},... | collective-permute-start | bytes 307208 | tf_op jit(solution)/shard_map/ppermute | solution.py:424
  7.0 3.0 %collective-permute-start.3 = (bf16[400,128]{1,0:T(8,128)(2,1)S(1)}, bf16[400,128]{1,0:T(8,128)(2,1)S(1)}, u32[]{:S(2)}, u32[]{:S(2)}) collective-permute-start(bf16[400,128]{1,0:T(8,128)(2,1)S(1)} %get-tuple-element.74), channel_id=1, source_target_pairs={{0,16},{1,17},{2,18},{3,19},{4,20},{5,21},{6,22},{7,23},{8,24},{9,... | collective-permute-start | bytes 307208 | tf_op jit(solution)/shard_map/ppermute | solution.py:424
  11.2 3.6 %collective-permute-start.5 = (bf16[400,128]{1,0:T(8,128)(2,1)S(1)}, bf16[400,128]{1,0:T(8,128)(2,1)S(1)}, u32[]{:S(2)}, u32[]{:S(2)}) collective-permute-start(bf16[400,128]{1,0:T(8,128)(2,1)S(1)} %get-tuple-element.76), channel_id=1, source_target_pairs={{0,24},{1,25},{2,26},{3,27},{4,28},{5,29},{6,30},{7,31},{8,16},{9,... | collective-permute-start | bytes 307208 | tf_op jit(solution)/shard_map/ppermute | solution.py:424
  15.7 2.8 %shard_map.137 = (f32[4,128,128]{2,1,0:T(8,128)S(1)}, f32[4,2,128,128]{3,2,1,0:T(8,128)S(1)}) custom-call(s32[2]{0:T(128)S(1)} %pad_add_fusion.me_ref, f32[16]{0:T(128)S(1)} %copy-done.6, bf16[400,128]{1,0:T(8,128)(2,1)S(1)} %get-tuple-element.69.refs_0_, bf16[400,128]{1,0:T(8,128)(2,1)S(1)} %collective-permute-done.1.refs_1_, ...), custom_call_target="tpu_custom_call" | custom-call | flops 30000000 | bytes 6000000 | tf_op jit(solution)/shard_map/pallas_call | solution.py:480
  18.5 7.2 %collective-permute-done.4.refs_5_ = bf16[400,128]{1,0:T(8,128)(2,1)S(1)} collective-permute-done((bf16[400,128]{1,0:T(8,128)(2,1)S(1)}, bf16[400,128]{1,0:T(8,128)(2,1)S(1)}, u32[]{:S(2)}, u32[]{:S(2)}) %collective-permute-start.4) | collective-permute-done | bytes 102432 | tf_op jit(solution)/shard_map/ppermute | solution.py:424
  25.7 6.2 %shard_map.138 = bf16[8,128,128]{2,1,0:T(8,128)(2,1)} custom-call(s32[2]{0:T(128)S(1)} %pad_add_fusion.me_ref, f32[16]{0:T(128)S(1)} %copy-done.6, f32[4,128,128]{2,1,0:T(8,128)S(1)} %get-tuple-element.72.near_ref, f32[4,2,128,128]{3,2,1,0:T(8,128)S(1)} %get-tuple-element.73.near_carry_ref, bf16[400,128]{1,0:T(8,128)(2,1)S(1)} %get-tuple-element.69.refs_0_, ...), custom_call_target="tpu_custom_call" | custom-call | flops 90000000 | bytes 18000000 | tf_op jit(solution)/shard_map/pallas_call | solution.py:488
  31.8 6.6 %all-to-all-start = ((bf16[8,128,128]{2,1,0:T(8,128)(2,1)}), bf16[8,128,128]{2,1,0:T(8,128)(2,1)S(1)}, u32[]{:S(2)}, u32[]{:S(2)}) async-start(bf16[8,128,128]{2,1,0:T(8,128)(2,1)} %shard_map.138), calls=%async_computation | async-start | bytes 524288 | tf_op jit(solution)/shard_map/all_to_all | solution.py:502
  38.4 3.7 %shard_map.139 = (bf16[1024,2048]{1,0:T(8,128)(2,1)S(1)}, bf16[1,128,2048]{2,1,0:T(8,128)(2,1)S(1)}, f32[1,1024]{1,0:T(1,128)S(1)}, f32[1,2048]{1,0:T(1,128)S(1)}, bf16[1,1024,2048]{2,1,0:T(8,128)(2,1)S(1)}) custom-call(bf16[1024,2048]{1,0:T(8,128)(2,1)} %refs_0_.1, bf16[1,128,2048]{2,1,0:T(8,128)(2,1)} %refs_1_.1, f32[1,1024]{1,0:T(1,128)} %bitcast.9, ...), custom_call_target="tpu_custom_call" | custom-call | flops 75000000 | bytes 15000000 | tf_op jit(solution)/shard_map/pallas_call | solution.py:466
  42.1 2.0 %copy-done.2 = bf16[1,1024,2048]{2,1,0:T(8,128)(2,1)} copy-done((bf16[1,1024,2048]{2,1,0:T(8,128)(2,1)}, bf16[1,1024,2048]{2,1,0:T(8,128)(2,1)S(1)}, u32[]{:S(2)}) %copy-start.2) | copy-done | bytes 4194328
  44.1 2.0 %copy-done.4 = bf16[1024,2048]{1,0:T(8,128)(2,1)} copy-done((bf16[1024,2048]{1,0:T(8,128)(2,1)}, bf16[1024,2048]{1,0:T(8,128)(2,1)S(1)}, u32[]{:S(2)}) %copy-start.4) | copy-done | bytes 4194328
  46.9 2.2 %copy-done.5 = bf16[1024,2048]{1,0:T(8,128)(2,1)S(1)} copy-done((bf16[1024,2048]{1,0:T(8,128)(2,1)S(1)}, bf16[1024,2048]{1,0:T(8,128)(2,1)}, u32[]{:S(2)}) %copy-start.5) | copy-done | bytes 4194328
  51.8 2.4 %collective-permute-start.35 = (bf16[64,2048]{1,0:T(8,128)(2,1)S(1)}, bf16[64,2048]{1,0:T(8,128)(2,1)S(1)}, u32[]{:S(2)}, u32[]{:S(2)}) collective-permute-start(bf16[64,2048]{1,0:T(8,128)(2,1)S(1)} %get-tuple-element.118), channel_id=1, source_target_pairs={{0,16},{1,17},{2,18},{3,19},{4,20},{5,21},{6,22},{7,23},{8,24},{9,... | collective-permute-start | bytes 786440 | tf_op jit(solution)/shard_map/ppermute | solution.py:424
  55.0 6.2 %collective-permute-done.7.refs_0_ = bf16[64,2048]{1,0:T(8,128)(2,1)S(1)} collective-permute-done((bf16[64,2048]{1,0:T(8,128)(2,1)S(1)}, bf16[64,2048]{1,0:T(8,128)(2,1)S(1)}, u32[]{:S(2)}, u32[]{:S(2)}) %collective-permute-start.7) | collective-permute-done | bytes 262176 | tf_op jit(solution)/shard_map/ppermute | solution.py:424
  61.5 1.6 %collective-permute-start.8 = (bf16[32,2048]{1,0:T(8,128)(2,1)S(1)}, bf16[32,2048]{1,0:T(8,128)(2,1)S(1)}, u32[]{:S(2)}, u32[]{:S(2)}) collective-permute-start(bf16[32,2048]{1,0:T(8,128)(2,1)S(1)} %get-tuple-element.85), channel_id=1, source_target_pairs={{0,2},{1,3},{2,0},{3,1},{4,6},{5,7},{6,4},{7,5},{8,10},{9,11},{10,... | collective-permute-start | bytes 393224 | tf_op jit(solution)/shard_map/ppermute | solution.py:424
  63.0 1.8 %collective-permute-start.9 = (bf16[32,2048]{1,0:T(8,128)(2,1)S(1)}, bf16[32,2048]{1,0:T(8,128)(2,1)S(1)}, u32[]{:S(2)}, u32[]{:S(2)}) collective-permute-start(bf16[32,2048]{1,0:T(8,128)(2,1)S(1)} %get-tuple-element.86), channel_id=1, source_target_pairs={{0,4},{1,5},{2,6},{3,7},{4,0},{5,1},{6,2},{7,3},{8,12},{9,13},{10,... | collective-permute-start | bytes 393224 | tf_op jit(solution)/shard_map/ppermute | solution.py:424
  65.0 8.1 %collective-permute-done.35.refs_0_ = bf16[64,2048]{1,0:T(8,128)(2,1)S(1)} collective-permute-done((bf16[64,2048]{1,0:T(8,128)(2,1)S(1)}, bf16[64,2048]{1,0:T(8,128)(2,1)S(1)}, u32[]{:S(2)}, u32[]{:S(2)}) %collective-permute-start.35) | collective-permute-done | bytes 262176 | tf_op jit(solution)/shard_map/ppermute | solution.py:424
  73.4 1.6 %collective-permute-start.36 = (bf16[32,2048]{1,0:T(8,128)(2,1)S(1)}, bf16[32,2048]{1,0:T(8,128)(2,1)S(1)}, u32[]{:S(2)}, u32[]{:S(2)}) collective-permute-start(bf16[32,2048]{1,0:T(8,128)(2,1)S(1)} %get-tuple-element.120), channel_id=1, source_target_pairs={{0,2},{1,3},{2,0},{3,1},{4,6},{5,7},{6,4},{7,5},{8,10},{9,11},{10,... | collective-permute-start | bytes 393224 | tf_op jit(solution)/shard_map/ppermute | solution.py:424
  77.2 1.6 %collective-permute-start.27 = (bf16[32,2048]{1,0:T(8,128)(2,1)S(1)}, bf16[32,2048]{1,0:T(8,128)(2,1)S(1)}, u32[]{:S(2)}, u32[]{:S(2)}) collective-permute-start(bf16[32,2048]{1,0:T(8,128)(2,1)S(1)} %get-tuple-element.109), channel_id=1, source_target_pairs={{0,2},{1,3},{2,0},{3,1},{4,6},{5,7},{6,4},{7,5},{8,10},{9,11},{10,... | collective-permute-start | bytes 393224 | tf_op jit(solution)/shard_map/ppermute | solution.py:424
  87.6 3.0 %collective-permute-done.19.refs_2_ = bf16[32,2048]{1,0:T(8,128)(2,1)S(1)} collective-permute-done((bf16[32,2048]{1,0:T(8,128)(2,1)S(1)}, bf16[32,2048]{1,0:T(8,128)(2,1)S(1)}, u32[]{:S(2)}, u32[]{:S(2)}) %collective-permute-start.19) | collective-permute-done | bytes 131104 | tf_op jit(solution)/shard_map/ppermute | solution.py:424
  92.1 2.2 %copy-done.3 = bf16[1,1024,2048]{2,1,0:T(8,128)(2,1)S(1)} copy-done((bf16[1,1024,2048]{2,1,0:T(8,128)(2,1)S(1)}, bf16[1,1024,2048]{2,1,0:T(8,128)(2,1)}, u32[]{:S(2)}) %copy-start.3) | copy-done | bytes 4194328
  94.3 1.9 %shard_map.143 = (bf16[64,2048]{1,0:T(8,128)(2,1)S(1)}, bf16[64,2048]{1,0:T(8,128)(2,1)S(1)}) custom-call(bf16[32,2048]{1,0:T(8,128)(2,1)S(1)} %get-tuple-element.84.refs_0_, bf16[32,2048]{1,0:T(8,128)(2,1)S(1)} %collective-permute-done.8.refs_1_, bf16[32,2048]{1,0:T(8,128)(2,1)S(1)} %collective-permute-done.9.refs_2_, ...), custom_call_target="tpu_custom_call" | custom-call | flops 38400000 | bytes 7680000 | tf_op jit(solution)/shard_map/pallas_call | solution.py:514
  96.7 1.9 %shard_map.158 = (bf16[64,2048]{1,0:T(8,128)(2,1)S(1)}, bf16[64,2048]{1,0:T(8,128)(2,1)S(1)}) custom-call(bf16[32,2048]{1,0:T(8,128)(2,1)S(1)} %get-tuple-element.119.refs_0_, bf16[32,2048]{1,0:T(8,128)(2,1)S(1)} %collective-permute-done.36.refs_1_, bf16[32,2048]{1,0:T(8,128)(2,1)S(1)} %collective-permute-done.37.refs_2_, ...), custom_call_target="tpu_custom_call" | custom-call | flops 38400000 | bytes 7680000 | tf_op jit(solution)/shard_map/pallas_call | solution.py:514
  98.7 1.9 %shard_map.153 = (bf16[64,2048]{1,0:T(8,128)(2,1)S(1)}, bf16[64,2048]{1,0:T(8,128)(2,1)S(1)}) custom-call(bf16[32,2048]{1,0:T(8,128)(2,1)S(1)} %get-tuple-element.108.refs_0_, bf16[32,2048]{1,0:T(8,128)(2,1)S(1)} %collective-permute-done.27.refs_1_, bf16[32,2048]{1,0:T(8,128)(2,1)S(1)} %collective-permute-done.28.refs_2_, ...), custom_call_target="tpu_custom_call" | custom-call | flops 38400000 | bytes 7680000 | tf_op jit(solution)/shard_map/pallas_call | solution.py:514
  101.1 1.9 %shard_map.148 = (bf16[64,2048]{1,0:T(8,128)(2,1)S(1)}, bf16[64,2048]{1,0:T(8,128)(2,1)S(1)}) custom-call(bf16[32,2048]{1,0:T(8,128)(2,1)S(1)} %get-tuple-element.96.refs_0_, bf16[32,2048]{1,0:T(8,128)(2,1)S(1)} %collective-permute-done.18.refs_1_, bf16[32,2048]{1,0:T(8,128)(2,1)S(1)} %collective-permute-done.19.refs_2_, ...), custom_call_target="tpu_custom_call" | custom-call | flops 38400000 | bytes 7680000 | tf_op jit(solution)/shard_map/pallas_call | solution.py:514
  105.1 1.5 %collective-permute-start.15 = (bf16[32,2048]{1,0:T(8,128)(2,1)S(1)}, bf16[32,2048]{1,0:T(8,128)(2,1)S(1)}, u32[]{:S(2)}, u32[]{:S(2)}) collective-permute-start(bf16[32,2048]{1,0:T(8,128)(2,1)S(1)} %get-tuple-element.94), channel_id=1, source_target_pairs={{0,6},{1,7},{2,4},{3,5},{4,2},{5,3},{6,0},{7,1},{8,14},{9,15},{10,... | collective-permute-start | bytes 393224 | tf_op jit(solution)/shard_map/ppermute | solution.py:424
  111.0 2.0 %collective-permute-done.14.refs_3_ = bf16[32,2048]{1,0:T(8,128)(2,1)S(1)} collective-permute-done((bf16[32,2048]{1,0:T(8,128)(2,1)S(1)}, bf16[32,2048]{1,0:T(8,128)(2,1)S(1)}, u32[]{:S(2)}, u32[]{:S(2)}) %collective-permute-start.14) | collective-permute-done | bytes 131104 | tf_op jit(solution)/shard_map/ppermute | solution.py:424
  117.0 1.6 %collective-permute-done.42.refs_3_ = bf16[32,2048]{1,0:T(8,128)(2,1)S(1)} collective-permute-done((bf16[32,2048]{1,0:T(8,128)(2,1)S(1)}, bf16[32,2048]{1,0:T(8,128)(2,1)S(1)}, u32[]{:S(2)}, u32[]{:S(2)}) %collective-permute-start.42) | collective-permute-done | bytes 131104 | tf_op jit(solution)/shard_map/ppermute | solution.py:424
  119.7 4.7 %collective-permute-start.16 = (bf16[64,2048]{1,0:T(8,128)(2,1)S(1)}, bf16[64,2048]{1,0:T(8,128)(2,1)S(1)}, u32[]{:S(2)}, u32[]{:S(2)}) collective-permute-start(bf16[64,2048]{1,0:T(8,128)(2,1)S(1)} %shard_map.145), channel_id=1, source_target_pairs={{0,8},{1,9},{2,10},{3,11},{4,12},{5,13},{6,14},{7,15},{8,0},{9,1},... | collective-permute-start | bytes 786440 | tf_op jit(solution)/shard_map/ppermute | solution.py:424
  124.7 1.9 %collective-permute-start.44 = (bf16[64,2048]{1,0:T(8,128)(2,1)S(1)}, bf16[64,2048]{1,0:T(8,128)(2,1)S(1)}, u32[]{:S(2)}, u32[]{:S(2)}) collective-permute-start(bf16[64,2048]{1,0:T(8,128)(2,1)S(1)} %shard_map.160), channel_id=1, source_target_pairs={{0,16},{1,17},{2,18},{3,19},{4,20},{5,21},{6,22},{7,23},{8,24},{9,... | collective-permute-start | bytes 786440 | tf_op jit(solution)/shard_map/ppermute | solution.py:424
  130.5 4.9 %collective-permute-done.33.refs_3_ = bf16[32,2048]{1,0:T(8,128)(2,1)S(1)} collective-permute-done((bf16[32,2048]{1,0:T(8,128)(2,1)S(1)}, bf16[32,2048]{1,0:T(8,128)(2,1)S(1)}, u32[]{:S(2)}, u32[]{:S(2)}) %collective-permute-start.33) | collective-permute-done | bytes 131104 | tf_op jit(solution)/shard_map/ppermute | solution.py:424
  135.8 9.7 %collective-permute-done.44.refs_1_ = bf16[64,2048]{1,0:T(8,128)(2,1)S(1)} collective-permute-done((bf16[64,2048]{1,0:T(8,128)(2,1)S(1)}, bf16[64,2048]{1,0:T(8,128)(2,1)S(1)}, u32[]{:S(2)}, u32[]{:S(2)}) %collective-permute-start.44) | collective-permute-done | bytes 262176 | tf_op jit(solution)/shard_map/ppermute | solution.py:424
  (102 shorter events, 40.4 us)
Async XLA Ops:
  2.3 8.9 %collective-permute-start = (bf16[400,128]{1,0:T(8,128)(2,1)S(1)}, bf16[400,128]{1,0:T(8,128)(2,1)S(1)}, u32[]{:S(2)}, u32[]{:S(2)}) collective-permute-start(bf16[400,128]{1,0:T(8,128)(2,1)S(1)} %get-tuple-element.68), channel_id=1, source_target_pairs={{0,8},{1,9},{2,10},{3,11},{4,12},{5,13},{6,14},{7,15},{8,0},{9,1},... | collective-permute-start | bytes 307208 | tf_op jit(solution)/shard_map/ppermute | solution.py:424
  5.4 9.4 %collective-permute-start.1 = (bf16[400,128]{1,0:T(8,128)(2,1)S(1)}, bf16[400,128]{1,0:T(8,128)(2,1)S(1)}, u32[]{:S(2)}, u32[]{:S(2)}) collective-permute-start(bf16[400,128]{1,0:T(8,128)(2,1)S(1)} %get-tuple-element.70), channel_id=1, source_target_pairs={{0,4},{1,5},{2,6},{3,7},{4,0},{5,1},{6,2},{7,3},{8,12},{9,13},{10,... | collective-permute-start | bytes 307208 | tf_op jit(solution)/shard_map/ppermute | solution.py:424
  6.9 8.1 %collective-permute-start.2 = (bf16[400,128]{1,0:T(8,128)(2,1)S(1)}, bf16[400,128]{1,0:T(8,128)(2,1)S(1)}, u32[]{:S(2)}, u32[]{:S(2)}) collective-permute-start(bf16[400,128]{1,0:T(8,128)(2,1)S(1)} %get-tuple-element.71), channel_id=1, source_target_pairs={{0,12},{1,13},{2,14},{3,15},{4,8},{5,9},{6,10},{7,11},{8,4},{9,5},... | collective-permute-start | bytes 307208 | tf_op jit(solution)/shard_map/ppermute | solution.py:424
  7.0 11.5 %collective-permute-start.3 = (bf16[400,128]{1,0:T(8,128)(2,1)S(1)}, bf16[400,128]{1,0:T(8,128)(2,1)S(1)}, u32[]{:S(2)}, u32[]{:S(2)}) collective-permute-start(bf16[400,128]{1,0:T(8,128)(2,1)S(1)} %get-tuple-element.74), channel_id=1, source_target_pairs={{0,16},{1,17},{2,18},{3,19},{4,20},{5,21},{6,22},{7,23},{8,24},{9,... | collective-permute-start | bytes 307208 | tf_op jit(solution)/shard_map/ppermute | solution.py:424
  9.9 15.8 %collective-permute-start.4 = (bf16[400,128]{1,0:T(8,128)(2,1)S(1)}, bf16[400,128]{1,0:T(8,128)(2,1)S(1)}, u32[]{:S(2)}, u32[]{:S(2)}) collective-permute-start(bf16[400,128]{1,0:T(8,128)(2,1)S(1)} %get-tuple-element.75), channel_id=1, source_target_pairs={{0,20},{1,21},{2,22},{3,23},{4,16},{5,17},{6,18},{7,19},{8,28},{9,... | collective-permute-start | bytes 307208 | tf_op jit(solution)/shard_map/ppermute | solution.py:424
  11.2 14.5 %collective-permute-start.5 = (bf16[400,128]{1,0:T(8,128)(2,1)S(1)}, bf16[400,128]{1,0:T(8,128)(2,1)S(1)}, u32[]{:S(2)}, u32[]{:S(2)}) collective-permute-start(bf16[400,128]{1,0:T(8,128)(2,1)S(1)} %get-tuple-element.76), channel_id=1, source_target_pairs={{0,24},{1,25},{2,26},{3,27},{4,28},{5,29},{6,30},{7,31},{8,16},{9,... | collective-permute-start | bytes 307208 | tf_op jit(solution)/shard_map/ppermute | solution.py:424
  14.8 10.9 %collective-permute-start.6 = (bf16[400,128]{1,0:T(8,128)(2,1)S(1)}, bf16[400,128]{1,0:T(8,128)(2,1)S(1)}, u32[]{:S(2)}, u32[]{:S(2)}) collective-permute-start(bf16[400,128]{1,0:T(8,128)(2,1)S(1)} %get-tuple-element.77), channel_id=1, source_target_pairs={{0,28},{1,29},{2,30},{3,31},{4,24},{5,25},{6,26},{7,27},{8,20},{9,... | collective-permute-start | bytes 307208 | tf_op jit(solution)/shard_map/ppermute | solution.py:424
  31.8 15.1 %all-to-all-start = ((bf16[8,128,128]{2,1,0:T(8,128)(2,1)}), bf16[8,128,128]{2,1,0:T(8,128)(2,1)S(1)}, u32[]{:S(2)}, u32[]{:S(2)}) async-start(bf16[8,128,128]{2,1,0:T(8,128)(2,1)} %shard_map.138), calls=%async_computation | async-start | bytes 524288 | tf_op jit(solution)/shard_map/all_to_all | solution.py:502
  50.5 10.7 %collective-permute-start.7 = (bf16[64,2048]{1,0:T(8,128)(2,1)S(1)}, bf16[64,2048]{1,0:T(8,128)(2,1)S(1)}, u32[]{:S(2)}, u32[]{:S(2)}) collective-permute-start(bf16[64,2048]{1,0:T(8,128)(2,1)S(1)} %get-tuple-element.83), channel_id=1, source_target_pairs={{0,8},{1,9},{2,10},{3,11},{4,12},{5,13},{6,14},{7,15},{8,0},{9,1},... | collective-permute-start | bytes 786440 | tf_op jit(solution)/shard_map/ppermute | solution.py:424
  51.8 21.3 %collective-permute-start.35 = (bf16[64,2048]{1,0:T(8,128)(2,1)S(1)}, bf16[64,2048]{1,0:T(8,128)(2,1)S(1)}, u32[]{:S(2)}, u32[]{:S(2)}) collective-permute-start(bf16[64,2048]{1,0:T(8,128)(2,1)S(1)} %get-tuple-element.118), channel_id=1, source_target_pairs={{0,16},{1,17},{2,18},{3,19},{4,20},{5,21},{6,22},{7,23},{8,24},{9,... | collective-permute-start | bytes 786440 | tf_op jit(solution)/shard_map/ppermute | solution.py:424
  54.1 20.8 %collective-permute-start.17 = (bf16[64,2048]{1,0:T(8,128)(2,1)S(1)}, bf16[64,2048]{1,0:T(8,128)(2,1)S(1)}, u32[]{:S(2)}, u32[]{:S(2)}) collective-permute-start(bf16[64,2048]{1,0:T(8,128)(2,1)S(1)} %get-tuple-element.95), channel_id=1, source_target_pairs={{0,24},{1,25},{2,26},{3,27},{4,28},{5,29},{6,30},{7,31},{8,16},{9,... | collective-permute-start | bytes 786440 | tf_op jit(solution)/shard_map/ppermute | solution.py:424
  61.5 14.9 %collective-permute-start.8 = (bf16[32,2048]{1,0:T(8,128)(2,1)S(1)}, bf16[32,2048]{1,0:T(8,128)(2,1)S(1)}, u32[]{:S(2)}, u32[]{:S(2)}) collective-permute-start(bf16[32,2048]{1,0:T(8,128)(2,1)S(1)} %get-tuple-element.85), channel_id=1, source_target_pairs={{0,2},{1,3},{2,0},{3,1},{4,6},{5,7},{6,4},{7,5},{8,10},{9,11},{10,... | collective-permute-start | bytes 393224 | tf_op jit(solution)/shard_map/ppermute | solution.py:424
  63.0 14.2 %collective-permute-start.9 = (bf16[32,2048]{1,0:T(8,128)(2,1)S(1)}, bf16[32,2048]{1,0:T(8,128)(2,1)S(1)}, u32[]{:S(2)}, u32[]{:S(2)}) collective-permute-start(bf16[32,2048]{1,0:T(8,128)(2,1)S(1)} %get-tuple-element.86), channel_id=1, source_target_pairs={{0,4},{1,5},{2,6},{3,7},{4,0},{5,1},{6,2},{7,3},{8,12},{9,13},{10,... | collective-permute-start | bytes 393224 | tf_op jit(solution)/shard_map/ppermute | solution.py:424
  64.8 13.9 %collective-permute-start.10 = (bf16[32,2048]{1,0:T(8,128)(2,1)S(1)}, bf16[32,2048]{1,0:T(8,128)(2,1)S(1)}, u32[]{:S(2)}, u32[]{:S(2)}) collective-permute-start(bf16[32,2048]{1,0:T(8,128)(2,1)S(1)} %get-tuple-element.87), channel_id=1, source_target_pairs={{0,6},{1,7},{2,4},{3,5},{4,2},{5,3},{6,0},{7,1},{8,14},{9,15},{10,... | collective-permute-start | bytes 393224 | tf_op jit(solution)/shard_map/ppermute | solution.py:424
  74.9 7.0 %collective-permute-start.37 = (bf16[32,2048]{1,0:T(8,128)(2,1)S(1)}, bf16[32,2048]{1,0:T(8,128)(2,1)S(1)}, u32[]{:S(2)}, u32[]{:S(2)}) collective-permute-start(bf16[32,2048]{1,0:T(8,128)(2,1)S(1)} %get-tuple-element.121), channel_id=1, source_target_pairs={{0,4},{1,5},{2,6},{3,7},{4,0},{5,1},{6,2},{7,3},{8,12},{9,13},{10,... | collective-permute-start | bytes 393224 | tf_op jit(solution)/shard_map/ppermute | solution.py:424
  82.7 9.4 %collective-permute-start.11 = (bf16[64,2048]{1,0:T(8,128)(2,1)S(1)}, bf16[64,2048]{1,0:T(8,128)(2,1)S(1)}, u32[]{:S(2)}, u32[]{:S(2)}) collective-permute-start(bf16[64,2048]{1,0:T(8,128)(2,1)S(1)} %shard_map.142), channel_id=1, source_target_pairs={{0,1},{1,0},{2,3},{3,2},{4,5},{5,4},{6,7},{7,6},{8,9},{9,8},{10,11... | collective-permute-start | bytes 786440 | tf_op jit(solution)/shard_map/ppermute | solution.py:424
  82.8 13.9 %collective-permute-start.39 = (bf16[64,2048]{1,0:T(8,128)(2,1)S(1)}, bf16[64,2048]{1,0:T(8,128)(2,1)S(1)}, u32[]{:S(2)}, u32[]{:S(2)}) collective-permute-start(bf16[64,2048]{1,0:T(8,128)(2,1)S(1)} %shard_map.157), channel_id=1, source_target_pairs={{0,1},{1,0},{2,3},{3,2},{4,5},{5,4},{6,7},{7,6},{8,9},{9,8},{10,11... | collective-permute-start | bytes 786440 | tf_op jit(solution)/shard_map/ppermute | solution.py:424
  87.5 11.2 %collective-permute-start.30 = (bf16[64,2048]{1,0:T(8,128)(2,1)S(1)}, bf16[64,2048]{1,0:T(8,128)(2,1)S(1)}, u32[]{:S(2)}, u32[]{:S(2)}) collective-permute-start(bf16[64,2048]{1,0:T(8,128)(2,1)S(1)} %shard_map.152), channel_id=1, source_target_pairs={{0,1},{1,0},{2,3},{3,2},{4,5},{5,4},{6,7},{7,6},{8,9},{9,8},{10,11... | collective-permute-start | bytes 786440 | tf_op jit(solution)/shard_map/ppermute | solution.py:424
  92.0 9.1 %collective-permute-start.21 = (bf16[64,2048]{1,0:T(8,128)(2,1)S(1)}, bf16[64,2048]{1,0:T(8,128)(2,1)S(1)}, u32[]{:S(2)}, u32[]{:S(2)}) collective-permute-start(bf16[64,2048]{1,0:T(8,128)(2,1)S(1)} %shard_map.147), channel_id=1, source_target_pairs={{0,1},{1,0},{2,3},{3,2},{4,5},{5,4},{6,7},{7,6},{8,9},{9,8},{10,11... | collective-permute-start | bytes 786440 | tf_op jit(solution)/shard_map/ppermute | solution.py:424
  104.2 8.8 %collective-permute-start.14 = (bf16[32,2048]{1,0:T(8,128)(2,1)S(1)}, bf16[32,2048]{1,0:T(8,128)(2,1)S(1)}, u32[]{:S(2)}, u32[]{:S(2)}) collective-permute-start(bf16[32,2048]{1,0:T(8,128)(2,1)S(1)} %get-tuple-element.93), channel_id=1, source_target_pairs={{0,4},{1,5},{2,6},{3,7},{4,0},{5,1},{6,2},{7,3},{8,12},{9,13},{10,... | collective-permute-start | bytes 393224 | tf_op jit(solution)/shard_map/ppermute | solution.py:424
  105.1 8.9 %collective-permute-start.15 = (bf16[32,2048]{1,0:T(8,128)(2,1)S(1)}, bf16[32,2048]{1,0:T(8,128)(2,1)S(1)}, u32[]{:S(2)}, u32[]{:S(2)}) collective-permute-start(bf16[32,2048]{1,0:T(8,128)(2,1)S(1)} %get-tuple-element.94), channel_id=1, source_target_pairs={{0,6},{1,7},{2,4},{3,5},{4,2},{5,3},{6,0},{7,1},{8,14},{9,15},{10,... | collective-permute-start | bytes 393224 | tf_op jit(solution)/shard_map/ppermute | solution.py:424
  106.7 8.5 %collective-permute-start.41 = (bf16[32,2048]{1,0:T(8,128)(2,1)S(1)}, bf16[32,2048]{1,0:T(8,128)(2,1)S(1)}, u32[]{:S(2)}, u32[]{:S(2)}) collective-permute-start(bf16[32,2048]{1,0:T(8,128)(2,1)S(1)} %get-tuple-element.126), channel_id=1, source_target_pairs={{0,2},{1,3},{2,0},{3,1},{4,6},{5,7},{6,4},{7,5},{8,10},{9,11},{10,... | collective-permute-start | bytes 393224 | tf_op jit(solution)/shard_map/ppermute | solution.py:424
  107.8 10.8 %collective-permute-start.42 = (bf16[32,2048]{1,0:T(8,128)(2,1)S(1)}, bf16[32,2048]{1,0:T(8,128)(2,1)S(1)}, u32[]{:S(2)}, u32[]{:S(2)}) collective-permute-start(bf16[32,2048]{1,0:T(8,128)(2,1)S(1)} %get-tuple-element.127), channel_id=1, source_target_pairs={{0,4},{1,5},{2,6},{3,7},{4,0},{5,1},{6,2},{7,3},{8,12},{9,13},{10,... | collective-permute-start | bytes 393224 | tf_op jit(solution)/shard_map/ppermute | solution.py:424
  109.5 10.1 %collective-permute-start.43 = (bf16[32,2048]{1,0:T(8,128)(2,1)S(1)}, bf16[32,2048]{1,0:T(8,128)(2,1)S(1)}, u32[]{:S(2)}, u32[]{:S(2)}) collective-permute-start(bf16[32,2048]{1,0:T(8,128)(2,1)S(1)} %get-tuple-element.128), channel_id=1, source_target_pairs={{0,6},{1,7},{2,4},{3,5},{4,2},{5,3},{6,0},{7,1},{8,14},{9,15},{10,... | collective-permute-start | bytes 393224 | tf_op jit(solution)/shard_map/ppermute | solution.py:424
  113.0 11.7 %collective-permute-start.23 = (bf16[32,2048]{1,0:T(8,128)(2,1)S(1)}, bf16[32,2048]{1,0:T(8,128)(2,1)S(1)}, u32[]{:S(2)}, u32[]{:S(2)}) collective-permute-start(bf16[32,2048]{1,0:T(8,128)(2,1)S(1)} %get-tuple-element.103), channel_id=1, source_target_pairs={{0,2},{1,3},{2,0},{3,1},{4,6},{5,7},{6,4},{7,5},{8,10},{9,11},{10,... | collective-permute-start | bytes 393224 | tf_op jit(solution)/shard_map/ppermute | solution.py:424
  114.0 12.6 %collective-permute-start.24 = (bf16[32,2048]{1,0:T(8,128)(2,1)S(1)}, bf16[32,2048]{1,0:T(8,128)(2,1)S(1)}, u32[]{:S(2)}, u32[]{:S(2)}) collective-permute-start(bf16[32,2048]{1,0:T(8,128)(2,1)S(1)} %get-tuple-element.104), channel_id=1, source_target_pairs={{0,4},{1,5},{2,6},{3,7},{4,0},{5,1},{6,2},{7,3},{8,12},{9,13},{10,... | collective-permute-start | bytes 393224 | tf_op jit(solution)/shard_map/ppermute | solution.py:424
  115.2 11.4 %collective-permute-start.25 = (bf16[32,2048]{1,0:T(8,128)(2,1)S(1)}, bf16[32,2048]{1,0:T(8,128)(2,1)S(1)}, u32[]{:S(2)}, u32[]{:S(2)}) collective-permute-start(bf16[32,2048]{1,0:T(8,128)(2,1)S(1)} %get-tuple-element.105), channel_id=1, source_target_pairs={{0,6},{1,7},{2,4},{3,5},{4,2},{5,3},{6,0},{7,1},{8,14},{9,15},{10,... | collective-permute-start | bytes 393224 | tf_op jit(solution)/shard_map/ppermute | solution.py:424
  118.6 10.9 %collective-permute-start.32 = (bf16[32,2048]{1,0:T(8,128)(2,1)S(1)}, bf16[32,2048]{1,0:T(8,128)(2,1)S(1)}, u32[]{:S(2)}, u32[]{:S(2)}) collective-permute-start(bf16[32,2048]{1,0:T(8,128)(2,1)S(1)} %get-tuple-element.115), channel_id=1, source_target_pairs={{0,2},{1,3},{2,0},{3,1},{4,6},{5,7},{6,4},{7,5},{8,10},{9,11},{10,... | collective-permute-start | bytes 393224 | tf_op jit(solution)/shard_map/ppermute | solution.py:424
  119.7 26.4 %collective-permute-start.16 = (bf16[64,2048]{1,0:T(8,128)(2,1)S(1)}, bf16[64,2048]{1,0:T(8,128)(2,1)S(1)}, u32[]{:S(2)}, u32[]{:S(2)}) collective-permute-start(bf16[64,2048]{1,0:T(8,128)(2,1)S(1)} %shard_map.145), channel_id=1, source_target_pairs={{0,8},{1,9},{2,10},{3,11},{4,12},{5,13},{6,14},{7,15},{8,0},{9,1},... | collective-permute-start | bytes 786440 | tf_op jit(solution)/shard_map/ppermute | solution.py:424
  124.7 20.8 %collective-permute-start.44 = (bf16[64,2048]{1,0:T(8,128)(2,1)S(1)}, bf16[64,2048]{1,0:T(8,128)(2,1)S(1)}, u32[]{:S(2)}, u32[]{:S(2)}) collective-permute-start(bf16[64,2048]{1,0:T(8,128)(2,1)S(1)} %shard_map.160), channel_id=1, source_target_pairs={{0,16},{1,17},{2,18},{3,19},{4,20},{5,21},{6,22},{7,23},{8,24},{9,... | collective-permute-start | bytes 786440 | tf_op jit(solution)/shard_map/ppermute | solution.py:424
  127.0 19.1 %collective-permute-start.26 = (bf16[64,2048]{1,0:T(8,128)(2,1)S(1)}, bf16[64,2048]{1,0:T(8,128)(2,1)S(1)}, u32[]{:S(2)}, u32[]{:S(2)}) collective-permute-start(bf16[64,2048]{1,0:T(8,128)(2,1)S(1)} %shard_map.150), channel_id=1, source_target_pairs={{0,24},{1,25},{2,26},{3,27},{4,28},{5,29},{6,30},{7,31},{8,16},{9,... | collective-permute-start | bytes 786440 | tf_op jit(solution)/shard_map/ppermute | solution.py:424
  128.4 7.1 %collective-permute-start.33 = (bf16[32,2048]{1,0:T(8,128)(2,1)S(1)}, bf16[32,2048]{1,0:T(8,128)(2,1)S(1)}, u32[]{:S(2)}, u32[]{:S(2)}) collective-permute-start(bf16[32,2048]{1,0:T(8,128)(2,1)S(1)} %get-tuple-element.116), channel_id=1, source_target_pairs={{0,4},{1,5},{2,6},{3,7},{4,0},{5,1},{6,2},{7,3},{8,12},{9,13},{10,... | collective-permute-start | bytes 393224 | tf_op jit(solution)/shard_map/ppermute | solution.py:424
  (21 other events, 179.9 us)
